TPU v7x, 512 devices: a whole 4x8x8 slice. The times are simulated.
512 devices in a mesh: ep: 32 (over z, x), tp: 16 (over y, core).
Axes of the slice: x: 4, y: 8, z: 8, core: 2. Of those that a mesh axis runs over, the one named last changes fastest.
Arguments:
- mixer_input_rows: bfloat16 [4096, 2048], P('ep'), may hold values from -6 to 6
- mix_gain: float32 [2048], replicated, may hold values from 0.1 to 1.9
- w_recept: bfloat16 [2048, 1024], P(None, 'tp'), may hold values from -0.125 to 0.125
- w_key: bfloat16 [2048, 1024], P(None, 'tp'), may hold values from -0.125 to 0.125
- w_value: bfloat16 [2048, 1024], P(None, 'tp'), may hold values from -0.125 to 0.125
- lowered_map_factor: bfloat16 [2048, 64], replicated, may hold values from -0.125 to 0.125
- decay_up: bfloat16 [64, 1024], P(None, 'tp'), may hold values from -0.75 to 0.75
- rate_up: bfloat16 [64, 1024], P(None, 'tp'), may hold values from -0.75 to 0.75
- decay_base: float32 [1024], P('tp'), may hold values from -13 to -2
- rate_base: float32 [1024], P('tp'), may hold values from -9 to 1
- decay_shift: float32 [4096, 16], P('ep', 'tp'), may hold values from -0.7 to 0, as said below
- out_gain: float32 [1024], P('tp'), may hold values from 0.1 to 1.9
- w_output: bfloat16 [1024, 2048], P('tp'), may hold values from -0.1875 to 0.1875
- moe_rows: bfloat16 [4096, 2048], P('ep'), may hold values from -6 to 6
- moe_gain: float32 [2048], replicated, may hold values from 0.1 to 1.9
- routes: int32 [4096, 2], P('ep'), may hold values from 0 to 31, all different within a row; in each aligned block of 128 rows (0 to 127, 128 to 255, ...) at most 16 rows name the same one
- route_weight: float32 [4096, 2], P('ep'), may hold values from 0.1 to 1
- exp_gate: bfloat16 [32, 2048, 4096], P('ep', None, 'tp'), may hold values from -0.125 to 0.125
- exp_up: bfloat16 [32, 2048, 4096], P('ep', None, 'tp'), may hold values from -0.125 to 0.125
- exp_down: bfloat16 [32, 4096, 2048], P('ep', 'tp'), may hold values from -0.125 to 0.125
Outputs:
- mix_out: bfloat16 [4096, 2048], P(('ep', 'tp'))
- moe_out: bfloat16 [4096, 2048], P('ep', 'tp')
Inputs may be any that keep to these rules, and one draw needn't show every extreme that they name: `routes`: in each aligned block of 128 rows no expert is named more than 16 times, and in some block one expert is named exactly 16 times; the two entries of a row differ. `decay_shift`: at most zero.
All inputs are finite; a program needn't handle non-finite values.
Results may differ from a plain program's by a relative error of at most 0.02.
Values may be sent and summed in bfloat16 or wider, within the bound.
No kernel may reach another device: no remote copies, remote signals or barrier semaphores. Data moves between devices by JAX's collectives and lax.ppermute only.
A program may use at most 64 MiB of HBM per device.

v0:
```python
import math

import jax
import jax.numpy as jnp
from jax import lax
from jax.sharding import PartitionSpec as P

DECAY_SCALE = math.exp(-0.5)


def carried_in(shard, axis, combine, identity, reverse):
    devices, place = (lax.axis_size(axis), lax.axis_index(axis))
    everything = jax.tree.map(
        lambda part, kind: lax.all_gather(part.astype(kind), axis),
        shard,
        jax.tree.map(lambda a: jnp.bfloat16 if a.dtype == jnp.float32 else a.dtype, shard),
    )
    start = jax.tree.map(
        lambda part, zero: jnp.broadcast_to(jnp.asarray(zero, part.dtype), part.shape),
        shard,
        identity,
    )

    def step(k, before):
        at = devices - 1 - k if reverse else k
        reached = at > place if reverse else at < place
        new = combine(
            before, jax.tree.map(lambda part, own: part[at].astype(own.dtype), everything, shard)
        )
        return jax.tree.map(lambda a, b: jnp.where(reached, a, b), new, before)

    return lax.fori_loop(0, devices, step, start)


def row_norm(row_block, gain_vector):
    entries = row_block.astype(jnp.float32)
    factor = lax.rsqrt(jnp.mean(entries * entries, axis=-1, keepdims=True) + 1e-06)
    return (entries * factor * gain_vector).astype(jnp.bfloat16)


def compose(earlier, latter):
    first_p, first_q = earlier
    second_p, second_q = latter
    joined_p = jnp.einsum("...ij,...jk->...ik", first_p, second_p)
    merged_query = jnp.einsum("...ij,...jk->...ik", first_q, second_p) + second_q
    return (joined_p, merged_query)


def heads_of(normed_input, weight, head_count):
    product = jnp.dot(normed_input, weight, preferred_element_type=jnp.float32)
    rounded = lax.optimization_barrier(product.astype(jnp.bfloat16))
    return rounded.astype(jnp.float32).reshape(normed_input.shape[0], head_count, -1)


def apply_transition(matrix, decay_row, unit_row, learn_row):
    along_key = jnp.einsum("hij,hj->hi", matrix, unit_row)
    return (
        matrix * decay_row[:, None, :] - along_key[:, :, None] * (unit_row * learn_row)[:, None, :]
    )


def local_totals(sequence, eye_stack, reverse):

    def local_advance(carry, inputs):
        total_p, total_q = carry
        decay_row, unit_row, learn_row, key_row, value_row, recept_row = inputs
        total_p = apply_transition(total_p, decay_row, unit_row, learn_row)
        total_q = (
            apply_transition(total_q, decay_row, unit_row, learn_row)
            + value_row[:, :, None] * key_row[:, None, :]
        )
        return ((total_p, total_q), None)

    start = (eye_stack, jnp.zeros_like(eye_stack))
    totals, _ = lax.scan(local_advance, start, sequence, reverse=reverse)
    return totals


def read_states(incoming, sequence, reverse):

    def read_advance(memory, inputs):
        decay_row, unit_row, learn_row, key_row, value_row, recept_row = inputs
        memory = (
            apply_transition(memory, decay_row, unit_row, learn_row)
            + value_row[:, :, None] * key_row[:, None, :]
        )
        return (memory, jnp.einsum("hij,hj->hi", memory, recept_row))

    _, outputs = lax.scan(read_advance, incoming, sequence, reverse=reverse)
    return outputs


def route_tables(route_rows, weight_rows, expert_count, slot_count):
    route_list = route_rows.reshape(-1)
    onehot = (route_list[:, None] == jnp.arange(expert_count, dtype=jnp.int32)[None, :]).astype(
        jnp.int32
    )
    slot_index = jnp.sum((jnp.cumsum(onehot, axis=0) - onehot) * onehot, axis=1)
    target = (route_list * slot_count + slot_index).reshape(route_rows.shape)
    columns = jnp.arange(expert_count * slot_count, dtype=jnp.int32)
    matches = target[:, :, None] == columns[None, None, :]
    placing = jnp.sum(matches.astype(jnp.int32), axis=1).astype(jnp.bfloat16)
    rounded = weight_rows.astype(jnp.bfloat16)
    weighing = jnp.sum(jnp.where(matches, rounded[:, :, None], jnp.zeros((), jnp.bfloat16)), axis=1)
    return (placing, weighing)


def expert_hidden(slot_rows, gate_shard, up_shard):
    flattened = slot_rows.reshape(-1, slot_rows.shape[-1])
    gate_part = jnp.dot(flattened, gate_shard, preferred_element_type=jnp.float32)
    up_part = jnp.dot(flattened, up_shard, preferred_element_type=jnp.float32)
    hidden = (jax.nn.silu(gate_part) * up_part).astype(jnp.bfloat16)
    return hidden.reshape(slot_rows.shape[:-1] + (gate_shard.shape[1],))


def shards(
    mixer_input_rows,
    mix_gain,
    w_recept,
    w_key,
    w_value,
    lowered_map_factor,
    decay_up,
    rate_up,
    decay_base,
    rate_base,
    decay_shift,
    out_gain,
    w_output,
    moe_rows,
    moe_gain,
    routes,
    route_weight,
    exp_gate,
    exp_up,
    exp_down,
):
    tokens = mixer_input_rows.shape[0]
    head_count = decay_shift.shape[1]
    head_width = w_recept.shape[1] // head_count
    normed_input = row_norm(mixer_input_rows, mix_gain)
    recept_heads = heads_of(normed_input, w_recept, head_count)
    key_heads = heads_of(normed_input, w_key, head_count)
    value_heads = heads_of(normed_input, w_value, head_count)
    lowrank = jnp.tanh(
        jnp.dot(normed_input, lowered_map_factor, preferred_element_type=jnp.float32)
    ).astype(jnp.bfloat16)
    decay_pre = decay_base + jnp.dot(lowrank, decay_up, preferred_element_type=jnp.float32)
    log_decay = -DECAY_SCALE * jax.nn.sigmoid(decay_pre) + jnp.repeat(
        decay_shift, head_width, axis=1
    )
    learn_rate = jax.nn.sigmoid(
        rate_base + jnp.dot(lowrank, rate_up, preferred_element_type=jnp.float32)
    )
    decay_rate = jnp.exp(log_decay).reshape(tokens, head_count, head_width)
    learn_rate = learn_rate.reshape(tokens, head_count, head_width)
    unit_key = key_heads * lax.rsqrt(jnp.sum(key_heads * key_heads, axis=-1, keepdims=True) + 1e-06)
    sequence = (decay_rate, unit_key, learn_rate, key_heads, value_heads, recept_heads)
    eye_stack = jnp.broadcast_to(
        jnp.eye(head_width, dtype=jnp.float32), (head_count, head_width, head_width)
    )
    forward_p, forward_q = local_totals(sequence, eye_stack, False)
    backward_p, backward_q = local_totals(sequence, eye_stack, True)
    identity = (eye_stack, jnp.zeros_like(eye_stack))
    incoming_list = []
    for backward, totals in ((False, (forward_p, forward_q)), (True, (backward_p, backward_q))):
        _, carried_q = carried_in(totals, "ep", compose, identity, backward)
        incoming_list.append(carried_q)
    forward_in, backward_in = incoming_list
    mixed_out = read_states(forward_in, sequence, False) + read_states(backward_in, sequence, True)
    centre = mixed_out - jnp.mean(mixed_out, axis=-1, keepdims=True)
    scaled = centre * lax.rsqrt(jnp.mean(centre * centre, axis=-1, keepdims=True) + 1e-05)
    grouped = (
        (scaled * out_gain.reshape(head_count, head_width)).astype(jnp.bfloat16).reshape(tokens, -1)
    )
    mix_out = lax.psum_scatter(
        jnp.dot(grouped, w_output, preferred_element_type=jnp.float32).astype(jnp.bfloat16),
        "tp",
        scatter_dimension=0,
        tiled=True,
    )
    group_rows = moe_rows.shape[0]
    experts = lax.axis_size("ep")
    slots = 4 * group_rows // experts
    moe_normed = row_norm(moe_rows, moe_gain)
    placing, weighing = route_tables(routes, route_weight, experts, slots)
    buffer = lax.dot_general(
        placing, moe_normed, (((0,), (0,)), ((), ())), preferred_element_type=jnp.float32
    )
    buffer = buffer.astype(jnp.bfloat16).reshape(experts, slots, -1)
    gate_shard = exp_gate[0]
    up_shard = exp_up[0]
    down_shard = exp_down[0]
    arrived = lax.all_to_all(buffer, "ep", split_axis=0, concat_axis=0, tiled=True)
    hidden = expert_hidden(arrived, gate_shard, up_shard)
    partial_sum = jnp.dot(
        hidden.reshape(-1, hidden.shape[-1]), down_shard, preferred_element_type=jnp.float32
    )
    partial_sum = partial_sum.reshape(experts, slots, -1)
    summed = lax.psum_scatter(
        partial_sum.astype(jnp.bfloat16), "tp", scatter_dimension=2, tiled=True
    )
    returned = lax.all_to_all(summed, "ep", split_axis=0, concat_axis=0, tiled=True)
    moe_out = jnp.dot(
        weighing, returned.reshape(experts * slots, -1), preferred_element_type=jnp.float32
    )
    return (mix_out, moe_out.astype(jnp.bfloat16))


def solution(mesh):
    return jax.shard_map(
        shards,
        mesh=mesh,
        in_specs=(
            P("ep", None),
            P(),
            P(None, "tp"),
            P(None, "tp"),
            P(None, "tp"),
            P(),
            P(None, "tp"),
            P(None, "tp"),
            P("tp"),
            P("tp"),
            P("ep", "tp"),
            P("tp"),
            P("tp", None),
            P("ep", None),
            P(),
            P("ep", None),
            P("ep", None),
            P("ep", None, "tp"),
            P("ep", None, "tp"),
            P("ep", "tp", None),
        ),
        out_specs=(P(("ep", "tp"), None), P("ep", "tp")),
        check_vma=False,
    )
```

profile of v0, /device:TPU:31, one launch (start us, length us, event | category | flops | bytes accessed | tf_op | source)
XLA Modules:
  0.0 755.5 jit_solution(8333742480188175990)
XLA Ops:
  10.3 1.2 fusion.80
  11.5 3.2 convolution_convert_fusion.1
  14.7 13.0 %all-to-all-start = ((bf16[32,16,2048]{2,1,0:T(8,128)(2,1)}), bf16[32,16,2048]{2,1,0:T(8,128)(2,1)}, u32[]{:S(2)}, u32[]{:S(2)}) async-start(bf16[32,16,2048]{2,1,0:T(8,128)(2,1)} %bitcast.65), calls=%async_computation.1 | async-start | bytes 4194304 | tf_op jit(solution)/shard_map/all_to_all | solution.py:194
  30.4 52.4 %while.88 = (s32[]{:T(128)}, f32[1,64,64]{2,1,0:T(8,128)S(1)}, f32[1,64,64]{2,1,0:T(8,128)S(1)}, f32[128,1,64]{2,1,0:T(1,128)S(1)}, f32[128,1,64]{2,1,0:T(1,128)...) while((s32[]{:T(128)}, f32[1,64,64]{2,1,0:T(8,128)S(1)}, ...), condition=%wide.region_9.10_spmd, body=%wide.region_8.9_spmd.sunk | while | flops 49219 | bytes 136577 | solution.py:75
  82.8 37.1 %all-gather.2 = bf16[32,64,64]{2,1,0:T(8,128)(2,1)S(1)} all-gather(bf16[1,64,64]{2,1,0:T(8,128)(2,1)S(1)} %convert_element_type.130), channel_id=4, replica_groups=mesh['ep'=32,'tp'=16] {'ep'}, dimensions={0}, use_global_device_ids=true | all-gather | bytes 270336 | tf_op jit(solution)/shard_map/all_gather | solution.py:14
  120.0 36.2 %all-gather.3 = bf16[32,64,64]{2,1,0:T(8,128)(2,1)S(1)} all-gather(bf16[1,64,64]{2,1,0:T(8,128)(2,1)S(1)} %convert_element_type.131), channel_id=5, replica_groups=mesh['ep'=32,'tp'=16] {'ep'}, dimensions={0}, use_global_device_ids=true | all-gather | bytes 270336 | tf_op jit(solution)/shard_map/all_gather | solution.py:14
  156.2 9.9 %while.91 = (s32[]{:T(128)}, f32[1,64,64]{1,2,0:T(8,128)S(1)}, s32[]{:T(128)}, bf16[32,1,64,64]{3,2,1,0:T(8,128)(2,1)S(1)}, bf16[32,1,64,64]{3,2,0,1:T(8,128)(2,...) while((s32[]{:T(128)}, f32[1,64,64]{1,2,0:T(8,128)S(1)}, s32[]{:T(128)}, ...), condition=%wide.region_11.12_spmd.clone, body=%wide.region_10.11_spmd.clone.sunk | while | flops 544776 | bytes 182433 | solution.py:32
  166.7 60.6 %while.89 = (s32[]{:T(128)}, f32[1,64,64]{2,1,0:T(8,128)S(1)}, f32[128,1,64]{2,1,0:T(1,128)S(1)}, f32[128,1,64]{2,1,0:T(1,128)S(1)}, f32[128,1,64]{2,1,0:T(1,128...) while((s32[]{:T(128)}, f32[1,64,64]{2,1,0:T(8,128)S(1)}, ...), condition=%wide.region_13.14_spmd, body=%wide.region_12.13_spmd.sunk | while | flops 57411 | bytes 107397 | solution.py:89
  227.3 52.2 %while.86 = (s32[]{:T(128)}, f32[1,64,64]{2,1,0:T(8,128)S(1)}, f32[1,64,64]{2,1,0:T(8,128)S(1)}, f32[128,1,64]{2,1,0:T(1,128)S(1)}, f32[128,1,64]{2,1,0:T(1,128)...) while((s32[]{:T(128)}, f32[1,64,64]{2,1,0:T(8,128)S(1)}, ...), condition=%wide.region_3.4_spmd, body=%wide.region_2.3_spmd.sunk | while | flops 49218 | bytes 136557 | solution.py:75
  279.6 35.1 %all-gather = bf16[32,64,64]{2,1,0:T(8,128)(2,1)S(1)} all-gather(bf16[1,64,64]{2,1,0:T(8,128)(2,1)S(1)} %convert_element_type.127), channel_id=2, replica_groups=mesh['ep'=32,'tp'=16] {'ep'}, dimensions={0}, use_global_device_ids=true | all-gather | bytes 270336 | tf_op jit(solution)/shard_map/all_gather | solution.py:14
  314.7 36.4 %all-gather.1 = bf16[32,64,64]{2,1,0:T(8,128)(2,1)S(1)} all-gather(bf16[1,64,64]{2,1,0:T(8,128)(2,1)S(1)} %convert_element_type.128), channel_id=3, replica_groups=mesh['ep'=32,'tp'=16] {'ep'}, dimensions={0}, use_global_device_ids=true | all-gather | bytes 270336 | tf_op jit(solution)/shard_map/all_gather | solution.py:14
  351.0 9.8 %while.90 = (s32[]{:T(128)}, f32[1,64,64]{1,2,0:T(8,128)S(1)}, s32[]{:T(128)}, bf16[32,1,64,64]{3,2,1,0:T(8,128)(2,1)S(1)}, bf16[32,1,64,64]{3,2,0,1:T(8,128)(2,1)S(1)}, /*index=5*/s32[]{:T(128)}, s32[]{:T(128)}) while((s32[]{:T(128)}, f32[1,64,64]{1,2,0:T(8,128)S(1)}, s32[]{:T(128)}, bf16[32,1,64,64]{3,2,1,0:T(8,128)(2,1)S(1)}, ...), condition=%wide.region_5.6_spmd.clone, body=%wide.region_4.5_spmd.clone.sunk | while | flops 544772 | bytes 181863 | solution.py:32
  360.9 2.6 fusion.85
  363.5 2.3 fusion.62
  366.6 23.0 %copy.190 = bf16[32,16,2048]{1,0,2:T(8,128)(2,1)} copy(bf16[32,16,2048]{2,1,0:T(8,128)(2,1)S(1)} %convolution_convert_fusion) | data formatting | bytes 4194304
  389.5 28.7 %reshape.977 = bf16[2048,512]{1,0:T(8,128)(2,1)} reshape(bf16[2048,32,16]{2,1,0:T(8,128)(2,1)} %bitcast.406) | data formatting | bytes 4194304
  418.5 220.5 %while.87 = (s32[]{:T(128)}, f32[1,64,64]{2,1,0:T(8,128)S(1)}, f32[128,1,64]{2,1,0:T(1,128)S(1)}, f32[128,1,64]{2,1,0:T(1,128)S(1)}, f32[128,1,64]{2,1,0:T(1,128...) while((s32[]{:T(128)}, f32[1,64,64]{2,1,0:T(8,128)S(1)}, ...), condition=%wide.region_7.8_spmd, body=%wide.region_6.7_spmd.sunk | while | flops 57410 | bytes 107377 | solution.py:89
  434.9 0.9 fusion.210
  495.1 0.9 fusion.210
  520.8 0.9 fusion.210
  526.0 0.9 fusion.210
  562.3 0.9 fusion.210
  572.7 0.9 fusion.210
  598.5 0.9 fusion.210
  602.1 0.9 fusion.210
  632.9 0.9 fusion.210
  639.3 1.2 convolution_convert_fusion.2
  640.6 1.9 reshape.978
  642.4 1.7 copy.191
  644.1 7.6 %all-to-all-start.1 = ((bf16[32,16,128]{2,1,0:T(8,128)(2,1)}), bf16[32,16,128]{2,1,0:T(8,128)(2,1)S(1)}, u32[]{:S(2)}, u32[]{:S(2)}) async-start(bf16[32,16,128]{2,1,0:T(8,128)(2,1)} %copy.191), calls=%async_computation.2 | async-start | bytes 262144 | tf_op jit(solution)/shard_map/all_to_all | solution.py:203
  651.9 7.8 %all-to-all-done.1 = bf16[32,16,128]{2,1,0:T(8,128)(2,1)S(1)} async-done(((bf16[32,16,128]{2,1,0:T(8,128)(2,1)}), bf16[32,16,128]{2,1,0:T(8,128)(2,1)S(1)}, u32[]{:S(2)}, u32[]{:S(2)}) %all-to-all-start.1) | async-done | bytes 131104 | tf_op jit(solution)/shard_map/all_to_all | solution.py:203
  660.5 88.2 %reduce-scatter.5.cloned.1.call-done = bf16[8,2048]{1,0:T(8,128)(2,1)} async-done(((bf16[128,2048]{1,0:T(8,128)(2,1)}), bf16[8,2048]{1,0:T(8,128)(2,1)}) %reduce-scatter.5.cloned.1.call-update) | async-done | bytes 32784 | tf_op jit(solution)/shard_map/reduce_scatter | solution.py:176
  (2906 shorter events, 389.1 us)
Async XLA Ops:
  7.2 358.7 %copy-start = (bf16[1,256,2048]{2,1,0:T(8,128)(2,1)S(1)}, bf16[1,256,2048]{2,1,0:T(8,128)(2,1)}, u32[]{:S(2)}) copy-start(bf16[1,256,2048]{2,1,0:T(8,128)(2,1)} %param.51) | copy-start | bytes 3145732
  14.7 13.2 %copy-start.1 = (bf16[128,2048]{1,0:T(8,128)(2,1)S(1)}, bf16[128,2048]{1,0:T(8,128)(2,1)}, u32[]{:S(2)}) copy-start(bf16[128,2048]{1,0:T(8,128)(2,1)} %param.32) | copy-start | bytes 1572868
  14.7 13.4 %copy-start.7 = (bf16[2048,64]{0,1:T(8,128)(2,1)S(1)}, bf16[2048,64]{0,1:T(8,128)(2,1)}, u32[]{:S(2)}) copy-start(bf16[2048,64]{0,1:T(8,128)(2,1)} %param.35) | copy-start | bytes 786436
  14.7 13.4 %copy-start.13 = (f32[2048]{0:T(1024)S(1)}, f32[2048]{0:T(1024)}, u32[]{:S(2)}) copy-start(f32[2048]{0:T(1024)} %param.33) | copy-start | bytes 24580
  14.7 14.1 %copy-start.8 = (bf16[2048,64]{0,1:T(8,128)(2,1)S(1)}, bf16[2048,64]{0,1:T(8,128)(2,1)}, u32[]{:S(2)}) copy-start(bf16[2048,64]{0,1:T(8,128)(2,1)} %param.37) | copy-start | bytes 786436
  14.7 346.1 %all-to-all-start = ((bf16[32,16,2048]{2,1,0:T(8,128)(2,1)}), bf16[32,16,2048]{2,1,0:T(8,128)(2,1)}, u32[]{:S(2)}, u32[]{:S(2)}) async-start(bf16[32,16,2048]{2,1,0:T(8,128)(2,1)} %bitcast.65), calls=%async_computation.1 | async-start | bytes 4194304 | tf_op jit(solution)/shard_map/all_to_all | solution.py:194
  27.8 1.4 copy-start.11
  27.8 1.4 copy-start.15
  27.8 1.4 copy-start.16
  27.8 1.7 copy-start.12
  27.8 1.7 copy-start.17
  27.8 2.0 copy-start.9
  27.9 612.7 %reduce-scatter.7.cloned.1.call-start = ((), (), s32[]{:S(2)}) async-start(), calls=%async_computation.5 | async-start | bytes 2228224
  30.3 135.9 %copy-start.10 = (bf16[2048,64]{0,1:T(8,128)(2,1)S(1)}, bf16[2048,64]{0,1:T(8,128)(2,1)}, u32[]{:S(2)}) copy-start(bf16[2048,64]{0,1:T(8,128)(2,1)} %param.34) | copy-start | bytes 786436
  227.3 52.2 %copy-start.4 = (bf16[128,1,64]{2,1,0:T(2,128)(2,1)}, bf16[128,1,64]{2,1,0:T(2,128)(2,1)S(1)}, u32[]{:S(2)}) copy-start(bf16[128,1,64]{2,1,0:T(2,128)(2,1)S(1)} %get-tuple-element.1513) | copy-start | bytes 49156
  279.6 83.9 %copy-start.3 = (f32[128,1,64]{2,1,0:T(1,128)}, f32[128,1,64]{2,1,0:T(1,128)S(1)}, u32[]{:S(2)}) copy-start(f32[128,1,64]{2,1,0:T(1,128)S(1)} %get-tuple-element.1512) | copy-start | bytes 98308
  360.8 2.8 copy-start.6
  418.2 221.1 %copy-start.2 = (bf16[64,2048]{1,0:T(8,128)(2,1)S(1)}, bf16[64,2048]{1,0:T(8,128)(2,1)}, u32[]{:S(2)}) copy-start(bf16[64,2048]{1,0:T(8,128)(2,1)} %param.44) | copy-start | bytes 786436
  418.2 221.1 %copy-start.5 = (f32[64]{0:T(128)S(1)}, f32[64]{0:T(128)}, u32[]{:S(2)}) copy-start(f32[64]{0:T(128)} %param.43) | copy-start | bytes 772
  418.3 330.4 %reduce-scatter.5.cloned.1.call-start = ((), (), s32[]{:S(2)}) async-start(), calls=%async_computation.4 | async-start | bytes 557056 | tf_op jit(solution)/shard_map/reduce_scatter | solution.py:176
  639.1 12.6 %copy-start.14 = (f32[128,2]{0,1:T(2,128)S(1)}, f32[128,2]{0,1:T(2,128)}, u32[]{:S(2)}) copy-start(f32[128,2]{0,1:T(2,128)} %param.48) | copy-start | bytes 3076
  644.1 15.6 %all-to-all-start.1 = ((bf16[32,16,128]{2,1,0:T(8,128)(2,1)}), bf16[32,16,128]{2,1,0:T(8,128)(2,1)S(1)}, u32[]{:S(2)}, u32[]{:S(2)}) async-start(bf16[32,16,128]{2,1,0:T(8,128)(2,1)} %copy.191), calls=%async_computation.2 | async-start | bytes 262144 | tf_op jit(solution)/shard_map/all_to_all | solution.py:203
Sparse Core Ops, SparseCore 0:
  418.4 110.8 reduce-scatter.6
  640.7 107.9 reduce-scatter.4
where the time goes:
time: 758 us; the launch traced here: 756 us
  matrix products  256 us (34%)
  blocking collectives  145 us (19%)
  other arithmetic  141 us (19%)
  waiting for transfers between devices  96.1 us (13%)
  local copies, waits for them, and re-layouts  65.1 us (9%)
  starting transfers between devices  20.9 us (3%)
  loops' own time  16.6 us (2%)
  between operations  14.6 us (2%)
    all_gather x4, blocking collectives, carried_in(): lax.all_gather(part.astype(kind), axis)  145 us
    dot_general x256, matrix products, read_advance(): return (memory, jnp.einsum('hij,hj->hi', memory, recept_row))  136 us
    dot_general x768, matrix products, apply_transition(): along_key = jnp.einsum('hij,hj->hi', matrix, unit_row)  95.5 us
    reduce_scatter x1, waiting for transfers between devices, shards(): lax.psum_scatter(jnp.dot(grouped, w_output, preferred_element_type=jnp.fl...  88.2 us
    mul x512, other arithmetic, apply_transition(): matrix * decay_row[:, None, :]  86.1 us
    unnamed x42, local copies, waits for them, and re-layouts  56.2 us
    add x256, other arithmetic, local_advance(): apply_transition(total_q, decay_row, unit_row, learn_row)  29.5 us
    add x256, other arithmetic, read_advance(): apply_transition(memory, decay_row, unit_row, learn_row)  22.6 us
  transfers between devices with their start and end apart: 4, of which 2 were waited for; matrix products, arithmetic and copies ran while one was open for 53% of the time, Pallas kernels for 0%

commit v1 on v0

v1 whole, which is shorter than its diff:
```python
import functools
import math

import jax
import jax.numpy as jnp
from jax import lax
from jax.experimental import pallas as pl
from jax.experimental.pallas import tpu as pltpu
from jax.sharding import PartitionSpec as P


DECAY_SCALE = math.exp(-0.5)
HIGH = lax.Precision.HIGHEST
F32 = jnp.float32
BF16 = jnp.bfloat16
ROW = 4


def mm(a, b, precision=HIGH):
    return lax.dot_general(
        a, b, (((1,), (0,)), ((), ())), precision=precision, preferred_element_type=F32
    )


def mm_nt(a, b, precision=HIGH):
    return lax.dot_general(
        a, b, (((1,), (1,)), ((), ())), precision=precision, preferred_element_type=F32
    )


def mm_tn(a, b, precision=HIGH):
    return lax.dot_general(
        a, b, (((0,), (0,)), ((), ())), precision=precision, preferred_element_type=F32
    )


def norm_rows(rows, gain):
    entries = rows.astype(F32)
    factor = lax.rsqrt(jnp.mean(entries * entries, axis=-1, keepdims=True) + 1e-06)
    return (entries * factor * gain).astype(BF16)


def block_totals(log_decay, unit, rate, key, value, recept, reverse):
    tokens, width = log_decay.shape
    half = tokens // 2
    i = lax.broadcasted_iota(jnp.int32, (tokens, tokens), 0)
    j = lax.broadcasted_iota(jnp.int32, (tokens, tokens), 1)
    upto = (j >= i) if reverse else (j <= i)
    before = (j > i) if reverse else (j < i)
    same = (i // half) == (j // half)
    cum = mm(upto.astype(F32), log_decay)
    exc = cum - log_decay
    row = lax.broadcasted_iota(jnp.int32, (tokens, width), 0)
    if reverse:
        total = cum[:1]
        edge = cum[half : half + 1]
        first = row >= half
        mid_low, mid_high = (half // 2, half + half // 2)
    else:
        total = cum[tokens - 1 :]
        edge = cum[half - 1 : half]
        first = row < half
        mid_low, mid_high = (half // 2 - 1, half + half // 2 - 1)
    ref = jnp.where(row < half, cum[mid_low : mid_low + 1], cum[mid_high : mid_high + 1])
    learned = unit * rate
    down = jnp.exp(ref - cum)
    near_left = jnp.concatenate([unit * jnp.exp(exc - ref), recept * jnp.exp(cum - ref)], axis=0)
    near_right = jnp.concatenate([learned * down, key * down], axis=0)
    gone = jnp.full_like(cum, -1e30)
    far_down = jnp.exp(jnp.where(first, edge - cum, gone))
    far_left = jnp.concatenate(
        [
            unit * jnp.exp(jnp.where(first, gone, exc - edge)),
            recept * jnp.exp(jnp.where(first, gone, cum - edge)),
        ],
        axis=0,
    )
    far_right = jnp.concatenate([learned * far_down, key * far_down], axis=0)
    near = mm_nt(near_left, near_right)
    far = mm_nt(far_left, far_right)

    def part(up, left, mask):
        rows = slice(0, tokens) if up else slice(tokens, 2 * tokens)
        cols = slice(0, tokens) if left else slice(tokens, 2 * tokens)
        return jnp.where(mask, jnp.where(same, near[rows, cols], far[rows, cols]), 0.0)

    lower = part(True, True, before)
    unit_key = part(True, False, before)
    read_rank = part(False, True, upto)
    read_key = part(False, False, upto)
    eye = (i == j).astype(F32)
    inverse = eye - jnp.where((i // 2) == (j // 2), lower, 0.0)
    size = 2
    while size < half:
        link = jnp.where(((i // (2 * size)) == (j // (2 * size))) & ((i // size) != (j // size)), lower, 0.0)
        inverse = inverse - mm(inverse, mm(link, inverse))
        size *= 2
    written = mm(jnp.concatenate([unit_key, read_key], axis=0), value)
    right = jnp.concatenate([unit * jnp.exp(exc), written[:tokens]], axis=1)
    solved = mm(inverse, right)
    cross = jnp.where(same, 0.0, lower)
    solved = solved - mm(inverse, mm(cross, solved))
    reads = jnp.concatenate([recept * jnp.exp(cum), written[tokens:]], axis=1) - mm(read_rank, solved)
    tail = jnp.exp(total - cum)
    ki = lax.broadcasted_iota(jnp.int32, (width, width), 0)
    kj = lax.broadcasted_iota(jnp.int32, (width, width), 1)
    diag = jnp.where(ki == kj, jnp.broadcast_to(jnp.exp(total), (width, width)), 0.0)
    maps = jnp.concatenate([diag, mm_tn(key * tail, value)], axis=1) - mm_tn(learned * tail, solved)
    return reads, maps


def mixer_values(rows, gain, w_recept, w_key, w_value, w_low, decay_up, rate_up, decay_base, rate_base, shift):
    normed = norm_rows(rows, gain)

    def project(weight):
        return mm_nt(normed, weight, None).astype(BF16).astype(F32)

    recept, key, value = (project(w_recept), project(w_key), project(w_value))
    low = jnp.tanh(mm_nt(normed, w_low, None)).astype(BF16)
    tokens = rows.shape[0]
    i = lax.broadcasted_iota(jnp.int32, (tokens, tokens), 0)
    j = lax.broadcasted_iota(jnp.int32, (tokens, tokens), 1)
    shift = jnp.sum(jnp.where(i == j, shift, 0.0), axis=1, keepdims=True)
    log_decay = -DECAY_SCALE * jax.nn.sigmoid(decay_base + mm(low, decay_up, None)) + shift
    rate = jax.nn.sigmoid(rate_base + mm(low, rate_up, None))
    unit = key * lax.rsqrt(jnp.sum(key * key, axis=-1, keepdims=True) + 1e-06)
    ahead = block_totals(log_decay, unit, rate, key, value, recept, False)
    back = block_totals(log_decay, unit, rate, key, value, recept, True)
    return ahead, back


def mixer_kernel(*refs):
    ins, (reads_f, reads_b, maps) = refs[:11], refs[11:]
    ahead, back = mixer_values(*[ref[...] for ref in ins])
    reads_f[...] = ahead[0]
    reads_b[...] = back[0]
    width = ahead[1].shape[0]
    maps[:width] = ahead[1].astype(BF16)
    maps[width:] = back[1].astype(BF16)


def with_identity(maps):
    width = maps.shape[0]
    r = lax.broadcasted_iota(jnp.int32, maps.shape, 0)
    c = lax.broadcasted_iota(jnp.int32, maps.shape, 1)
    return jnp.concatenate([maps, (c == r + width).astype(maps.dtype)], axis=0)


def chained(blocks, reverse):
    level = blocks
    while len(level) > 1:
        last = len(level) == 2
        joined = []
        for k in range(0, len(level), 2):
            early, late = (level[k + 1], level[k]) if reverse else (level[k], level[k + 1])
            product = mm(late, with_identity(early), None)
            joined.append(product if last else product.astype(BF16))
        level = joined
    return level[0]


def plain_like(maps):
    r = lax.broadcasted_iota(jnp.int32, maps.shape, 0)
    c = lax.broadcasted_iota(jnp.int32, maps.shape, 1)
    return (r == c).astype(F32)


def kept(maps, use, plain):
    return jnp.where(use, maps.astype(F32), plain).astype(BF16)


def row_values(place, gathered):
    count = len(gathered)
    plain = plain_like(gathered[0][0])
    ahead, back = ([g[0] for g in gathered], [g[1] for g in gathered])
    before = chained([kept(ahead[k], k < place, plain) for k in range(count)], False)
    after = chained([kept(back[k], k > place, plain) for k in range(count)], True)
    return chained(ahead, False), chained(back, True), before, after


def row_kernel(place, high, *refs):
    held, (sent, before, after) = refs[:-3], refs[-3:]
    width = before.shape[0]
    count = len(held)
    held = [(r[:width], r[width:]) for r in held]
    at = place[0]
    gathered = []
    for k in range(count):
        far = lax.rem(at - k + count, count)
        chosen = []
        for side in range(2):
            value = held[0][side].astype(F32)
            for m in range(1, count):
                value = jnp.where(far == m, held[m][side].astype(F32), value)
            chosen.append(value.astype(BF16))
        gathered.append(chosen)
    total_f, total_b, before[...], after[...] = row_values(at, gathered)
    for k in range(sent.shape[0]):
        sent[k] = jnp.where(k > high[0], total_f, total_b).astype(BF16)


def output_values(place, core, arrived, before, after, reads_f, reads_b, gain, w_output, chips):
    count, width = len(arrived), before.shape[0]
    plain = plain_like(arrived[0])
    ahead = chained([kept(arrived[k], k < place, plain) for k in range(count)], False)
    back = chained([kept(arrived[k], k > place, plain) for k in range(count)], True)
    ahead = mm(before, with_identity(ahead))
    back = mm(after, with_identity(back))
    mixed = mm(reads_f, with_identity(ahead)) + mm(reads_b, with_identity(back))
    mixed = mixed[:, width:]
    centre = mixed - jnp.mean(mixed, axis=-1, keepdims=True)
    scaled = centre * lax.rsqrt(jnp.mean(centre * centre, axis=-1, keepdims=True) + 1e-05)
    grouped = scaled * gain
    split = grouped.reshape(chips, 2, -1, width)
    results = []
    for use in (core == 0, core != 0):
        rows = jnp.where(use, split[:, 0], split[:, 1]).reshape(-1, width)
        results.append(mm(rows.astype(BF16), w_output, None).astype(BF16))
    return results


def output_kernel(place, core, arrived, before, after, reads_f, reads_b, gain, w_output, own, away):
    values = output_values(
        place[0],
        core[0],
        [arrived[k] for k in range(arrived.shape[0])],
        before[...],
        after[...],
        reads_f[...],
        reads_b[...],
        gain[...],
        w_output[...],
        own.shape[0],
    )
    for out, value in zip((own, away), values):
        out[...] = value.reshape(out.shape)


def down_block(hidden, down, parity, width, y):
    columns = pl.ds(pl.multiple_of((2 * y + parity) * width, width), width)
    return mm(hidden, down[:, columns], None).astype(BF16)


def expert_kernel(width, core, arrived, swapped, gate, up, down, hidden, away):
    half = arrived.shape[1]
    at = core[0]
    near = pl.ds(pl.multiple_of(at * half, half), half)
    far = pl.ds(pl.multiple_of((1 - at) * half, half), half)
    pairs = [(arrived[...], near), (swapped[...], far)]
    gated = sum(mm(value, gate[where, :], None) for value, where in pairs)
    raised = sum(mm(value, up[where, :], None) for value, where in pairs)
    inner = (gated / (1.0 + jnp.exp(-gated)) * raised).astype(BF16)
    hidden[...] = inner
    for y in range(half // width):
        away[:, y * width : (y + 1) * width] = down_block(inner, down, 1 - at, width, y)


def pair_kernel(width, core, hidden, landed, down, out):
    inner = hidden[...]
    for y in range(out.shape[1] // width):
        columns = slice(y * width, (y + 1) * width)
        part = down_block(inner, down, core[0], width, y).astype(F32)
        out[:, columns] = (part + landed[:, columns].astype(F32)).astype(BF16)


def combine_kernel(returned, weighing, own, landed, out):
    chips, each, width = own.shape[0], own.shape[1], out.shape[2]
    tokens = weighing.shape[1]
    weighed = mm_tn(weighing[...], returned[...], None).astype(BF16)
    for y in range(chips):
        out[y, :tokens] = weighed[:, y * width : (y + 1) * width]
        joined = own[y].astype(F32) + landed[y].astype(F32)
        for k in range(own.shape[2] // width):
            rows = slice(tokens + k * each, tokens + (k + 1) * each)
            out[y, rows] = joined[:, k * width : (k + 1) * width].astype(BF16)


def finish_kernel(shares, mixed, moe):
    chips, width = shares.shape[0], shares.shape[2]
    tokens, each = moe.shape[0], mixed.shape[0]
    total = shares[0].astype(F32)
    for y in range(1, chips):
        total = total + shares[y].astype(F32)
    moe[...] = total[:tokens].astype(BF16)
    for k in range(mixed.shape[1] // width):
        rows = slice(tokens + k * each, tokens + (k + 1) * each)
        mixed[:, k * width : (k + 1) * width] = total[rows].astype(BF16)


def route_values(routes, weights, experts, slots):
    tokens = routes.shape[1]
    i = lax.broadcasted_iota(jnp.int32, (tokens, tokens), 0)
    j = lax.broadcasted_iota(jnp.int32, (tokens, tokens), 1)
    across = routes.astype(F32)
    along = weights.astype(BF16).astype(F32)
    expert = lax.broadcasted_iota(jnp.int32, (experts, tokens), 0).astype(F32)
    named = [(expert == across[k : k + 1]).astype(F32) for k in range(2)]
    earlier = mm((named[0] + named[1]).astype(BF16), (i < j).astype(BF16), None)
    row = lax.broadcasted_iota(jnp.int32, (experts * slots, tokens), 0).astype(F32)
    placing = jnp.zeros(row.shape, F32)
    weighing = jnp.zeros(row.shape, F32)
    for k in range(2):
        slot = jnp.sum(named[k] * earlier, axis=0, keepdims=True)
        match = row == across[k : k + 1] * slots + slot
        placing = placing + jnp.where(match, 1.0, 0.0)
        weighing = weighing + jnp.where(match, along[k : k + 1], 0.0)
    return placing.astype(BF16), weighing.astype(BF16)


def dispatch_kernel(experts, slots, core, rows, gain, routes, weights, buffer, weighing):
    placing, weigh = route_values(routes[...], weights[...], experts, slots)
    weighing[...] = weigh
    normed = norm_rows(rows[...], gain[...])
    width = normed.shape[1] // 2
    mine = jnp.where(core[0] == 0, normed[:, :width].astype(F32), normed[:, width:].astype(F32))
    buffer[...] = mm(placing, mine.astype(BF16), None).astype(BF16)


def call(kernel, outs, scalars, *args):
    smem = pl.BlockSpec(memory_space=pltpu.SMEM)
    vmem = pl.BlockSpec(memory_space=pltpu.VMEM)
    return pl.pallas_call(
        kernel,
        out_shape=outs,
        in_specs=[smem] * len(scalars) + [vmem] * len(args),
        out_specs=jax.tree.map(lambda _: vmem, outs),
    )(*scalars, *args)


def shards(
    mixer_input_rows,
    mix_gain,
    w_recept,
    w_key,
    w_value,
    lowered_map_factor,
    decay_up,
    rate_up,
    decay_base,
    rate_base,
    decay_shift,
    out_gain,
    w_output,
    moe_rows,
    moe_gain,
    routes,
    route_weight,
    exp_gate,
    exp_up,
    exp_down,
):
    experts, tp = (lax.axis_size("ep"), lax.axis_size("tp"))
    place, lane = (lax.axis_index("ep"), lax.axis_index("tp"))
    core = lane & 1
    chips = tp // 2
    across = ROW
    rows = experts // across
    high, low = (place // across, place % across)
    swap = [(k, k ^ 1) for k in range(tp)]
    tokens, model = moe_rows.shape
    slots = 4 * tokens // experts
    half = model // 2
    width = w_key.shape[1]
    piece = model // tp
    scalar = lambda v: v.astype(jnp.int32).reshape(1)
    shape = jax.ShapeDtypeStruct

    buffer, weighing = call(
        functools.partial(dispatch_kernel, experts, slots),
        (shape((experts * slots, half), BF16), shape((experts * slots, tokens), BF16)),
        (scalar(core),),
        moe_rows,
        moe_gain.reshape(1, -1),
        routes.T,
        route_weight.T,
    )
    arrived = lax.all_to_all(
        buffer.reshape(experts, slots, half), "ep", split_axis=0, concat_axis=0, tiled=True
    ).reshape(experts * slots, half)

    reads = shape((tokens, 2 * width), F32)
    wide = shape((width, 2 * width), F32)
    reads_f, reads_b, both = call(
        mixer_kernel,
        (reads, reads, shape((2 * width, 2 * width), BF16)),
        (),
        mixer_input_rows,
        mix_gain.reshape(1, -1),
        w_recept.T,
        w_key.T,
        w_value.T,
        lowered_map_factor.T,
        decay_up,
        rate_up,
        decay_base.reshape(1, -1),
        rate_base.reshape(1, -1),
        decay_shift.T,
    )

    others = [
        lax.ppermute(
            both,
            "ep",
            [(k, k // across * across + (k + m) % across) for k in range(experts)],
        )
        for m in range(1, across)
    ]
    sent, before, after = call(
        row_kernel,
        (shape((rows, width, 2 * width), BF16), wide, wide),
        (scalar(low), scalar(high)),
        both,
        *others,
    )

    arrived, sent = lax.optimization_barrier((arrived, sent))

    carried = lax.all_to_all(
        sent,
        "ep",
        split_axis=0,
        concat_axis=0,
        tiled=True,
        axis_index_groups=[[z * across + x for z in range(rows)] for x in range(across)],
    )

    swapped = lax.ppermute(arrived, "tp", swap)
    inner = exp_gate.shape[2]
    hidden, away = call(
        functools.partial(expert_kernel, piece),
        (shape((experts * slots, inner), BF16), shape((experts * slots, half), BF16)),
        (scalar(core),),
        arrived,
        swapped,
        exp_gate[0],
        exp_up[0],
        exp_down[0],
    )
    landed = lax.ppermute(away, "tp", swap)
    paired = call(
        functools.partial(pair_kernel, piece),
        shape((experts * slots, half), BF16),
        (scalar(core),),
        hidden,
        landed,
        exp_down[0],
    )

    returned = lax.all_to_all(
        paired.reshape(experts, slots, half), "ep", split_axis=0, concat_axis=0, tiled=True
    ).reshape(experts * slots, half)

    shares = shape((chips, tokens // tp, model), BF16)
    own_rows, away_rows = call(
        output_kernel,
        (shares, shares),
        (scalar(high), scalar(core)),
        carried,
        before,
        after,
        reads_f,
        reads_b,
        out_gain.reshape(1, -1),
        w_output,
    )
    landed_rows = lax.ppermute(away_rows, "tp", swap)

    parts = call(
        combine_kernel,
        shape((chips, 2 * tokens, piece), BF16),
        (),
        returned,
        weighing,
        own_rows,
        landed_rows,
    )
    parts = lax.all_to_all(
        parts,
        "tp",
        split_axis=0,
        concat_axis=0,
        tiled=True,
        axis_index_groups=[[2 * y + c for y in range(chips)] for c in range(2)],
    )
    mix_out, moe_out = call(
        finish_kernel,
        (shape((tokens // tp, model), BF16), shape((tokens, piece), BF16)),
        (),
        parts,
    )
    return (mix_out, moe_out)


def solution(mesh):
    return jax.shard_map(
        shards,
        mesh=mesh,
        in_specs=(
            P("ep", None),
            P(),
            P(None, "tp"),
            P(None, "tp"),
            P(None, "tp"),
            P(),
            P(None, "tp"),
            P(None, "tp"),
            P("tp"),
            P("tp"),
            P("ep", "tp"),
            P("tp"),
            P("tp", None),
            P("ep", None),
            P(),
            P("ep", None),
            P("ep", None),
            P("ep", None, "tp"),
            P("ep", None, "tp"),
            P("ep", "tp", None),
        ),
        out_specs=(P(("ep", "tp"), None), P("ep", "tp")),
        check_vma=False,
    )
```

time: 758 us -> 136 us (0.18)
  the two profiles are of different devices: /device:TPU:31 before, /device:TPU:4 now
where the time goes in v1:
time: 136 us; the launch traced here: 135 us
  starting transfers between devices  38.7 us (28%)
  waiting for transfers between devices  36.1 us (27%)
  Pallas kernels  32.4 us (24%)
  blocking collectives  23.2 us (17%)
  local copies, waits for them, and re-layouts  4.19 us (3%)
    pallas_call x8, Pallas kernels, call(): pl.pallas_call(kernel, out_shape=outs, in_specs=[smem] * len(scalars) + [...  32.4 us
    all_to_all x1, blocking collectives, shards(): lax.all_to_all(parts, 'tp', split_axis=0, concat_axis=0, tiled=True, axis...  23.2 us
    all_to_all x1, waiting for transfers between devices, shards(): lax.all_to_all(paired.reshape(experts, slots, half), 'ep', split_axis=0,...  20.6 us
    all_to_all x1, starting transfers between devices, shards(): lax.all_to_all(buffer.reshape(experts, slots, half), 'ep', split_axis=0,...  13.4 us
    ppermute x3, starting transfers between devices, shards(): lax.ppermute(both, 'ep', [(k, k // across * across + (k + m) % across) fo...  8.55 us
    all_to_all x1, starting transfers between devices, shards(): lax.all_to_all(paired.reshape(experts, slots, half), 'ep', split_axis=0,...  6.38 us
    all_to_all x1, waiting for transfers between devices, shards(): lax.all_to_all(sent, 'ep', split_axis=0, concat_axis=0, tiled=True, axis_...  5.28 us
    all_to_all x1, starting transfers between devices, shards(): lax.all_to_all(sent, 'ep', split_axis=0, concat_axis=0, tiled=True, axis_...  4.46 us
  transfers between devices with their start and end apart: 9, of which 7 were waited for; matrix products, arithmetic and copies ran while one was open for 0% of the time, Pallas kernels for 15%

profile of v1, /device:TPU:4, one launch (start us, length us, event | category | flops | bytes accessed | tf_op | source)
XLA Modules:
  0.0 135.4 jit_solution(10591294063293540091)
XLA Ops:
  0.6 2.7 %shard_map.203 = (bf16[512,1024]{1,0:T(8,128)(2,1)}, bf16[512,128]{1,0:T(8,128)(2,1)}) custom-call(s32[1]{0:T(128)} %bitcast.core, bf16[128,2048]{1,0:T(8,128)(2,1)} %rows.1, f32[1,2048]{1,0:T(1,128)} %bitcast.35, s32[2,128]{1,0:T(2,128)} %bitcast.37, f32[2,128]{1,0:T(2,128)} %bitcast.38), custom_call_target="tpu_custom_call" | custom-call | tf_op jit(solution)/shard_map/pallas_call | solution.py:322
  3.4 13.4 %all-to-all-start = ((bf16[32,16,1024]{2,1,0:T(8,128)(2,1)}), bf16[32,16,1024]{2,1,0:T(8,128)(2,1)S(1)}, u32[]{:S(2)}, u32[]{:S(2)}) async-start(bf16[32,16,1024]{2,1,0:T(8,128)(2,1)} %bitcast.28), calls=%async_computation | async-start | bytes 2097152 | tf_op jit(solution)/shard_map/all_to_all | solution.py:377
  16.8 10.7 %shard_map.204 = (f32[128,128]{1,0:T(8,128)}, f32[128,128]{1,0:T(8,128)}, bf16[128,128]{1,0:T(8,128)(2,1)}) custom-call(bf16[128,2048]{1,0:T(8,128)(2,1)} %refs_0_.1, f32[1,2048]{1,0:T(1,128)} %bitcast.36, bf16[64,2048]{1,0:T(8,128)(2,1)} %bitcast.31, bf16[64,2048]{1,0:T(8,128)(2,1)} %bitcast.32, bf16[64,2048]{1,0:T(8,128)(2,1)} %bitcast.33, ...), custom_call_target="tpu_custom_call" | custom-call | tf_op jit(solution)/shard_map/pallas_call | solution.py:322
  27.5 3.0 %collective-permute-start = (bf16[128,128]{1,0:T(8,128)(2,1)}, bf16[128,128]{1,0:T(8,128)(2,1)S(1)}, u32[]{:S(2)}, u32[]{:S(2)}) collective-permute-start(bf16[128,128]{1,0:T(8,128)(2,1)} %get-tuple-element.17.refs_0_), channel_id=1, source_target_pairs={{0,16},{16,32},{32,48},{48,0},{64,80},{80,96},{96,112},{112,64},{1... | collective-permute-start | bytes 98312 | tf_op jit(solution)/shard_map/ppermute | solution.py:401
  30.6 2.8 %collective-permute-start.1 = (bf16[128,128]{1,0:T(8,128)(2,1)}, bf16[128,128]{1,0:T(8,128)(2,1)S(1)}, u32[]{:S(2)}, u32[]{:S(2)}) collective-permute-start(bf16[128,128]{1,0:T(8,128)(2,1)} %get-tuple-element.17.refs_0_), channel_id=1, source_target_pairs={{0,32},{16,48},{32,0},{48,16},{64,96},{80,112},{96,64},{112,80},{1... | collective-permute-start | bytes 98312 | tf_op jit(solution)/shard_map/ppermute | solution.py:401
  33.4 2.7 %collective-permute-start.2 = (bf16[128,128]{1,0:T(8,128)(2,1)}, bf16[128,128]{1,0:T(8,128)(2,1)S(1)}, u32[]{:S(2)}, u32[]{:S(2)}) collective-permute-start(bf16[128,128]{1,0:T(8,128)(2,1)} %get-tuple-element.17.refs_0_), channel_id=1, source_target_pairs={{0,48},{16,0},{32,16},{48,32},{64,112},{80,64},{96,80},{112,96},{1... | collective-permute-start | bytes 98312 | tf_op jit(solution)/shard_map/ppermute | solution.py:401
  36.2 0.0 copy-start.6
  36.2 2.5 %collective-permute-done.1.refs_2_ = bf16[128,128]{1,0:T(8,128)(2,1)S(1)} collective-permute-done((bf16[128,128]{1,0:T(8,128)(2,1)}, bf16[128,128]{1,0:T(8,128)(2,1)S(1)}, u32[]{:S(2)}, u32[]{:S(2)}) %collective-permute-start.1) | collective-permute-done | bytes 32800 | tf_op jit(solution)/shard_map/ppermute | solution.py:401
  38.6 0.9 collective-permute-done.2.refs_3_
  39.5 0.6 copy-done.8
  40.1 2.2 %shard_map.205 = (bf16[8,64,128]{2,1,0:T(8,128)(2,1)}, f32[64,128]{1,0:T(8,128)}, f32[64,128]{1,0:T(8,128)}) custom-call(s32[1]{0:T(128)} %bitcast.6.place, s32[1]{0:T(128)} %bitcast.7.high.place, bf16[128,128]{1,0:T(8,128)(2,1)} %get-tuple-element.17.refs_0_, bf16[128,128]{1,0:T(8,128)(2,1)} %copy-done.6, bf16[128,128]{1,0:T(8,128)(2,1)} %copy-done.7, ...), custom_call_target="tpu_custom_call" | custom-call | tf_op jit(solution)/shard_map/pallas_call | solution.py:322
  42.3 2.6 %all-to-all-done = bf16[32,16,1024]{2,1,0:T(8,128)(2,1)S(1)} async-done(((bf16[32,16,1024]{2,1,0:T(8,128)(2,1)}), bf16[32,16,1024]{2,1,0:T(8,128)(2,1)S(1)}, u32[]{:S(2)}, u32[]{:S(2)}) %all-to-all-start) | async-done | bytes 1048608 | tf_op jit(solution)/shard_map/all_to_all | solution.py:377
  44.9 1.9 %collective-permute-start.3 = (bf16[512,1024]{1,0:T(8,128)(2,1)S(1)}, bf16[512,1024]{1,0:T(8,128)(2,1)S(1)}, u32[]{:S(2)}, u32[]{:S(2)}) collective-permute-start(bf16[512,1024]{1,0:T(8,128)(2,1)S(1)} %bitcast.26), channel_id=1, source_target_pairs={{0,1},{1,0},{2,3},{3,2},{4,5},{5,4},{6,7},{7,6},{8,9},{9,8},{10,11... | collective-permute-start | bytes 3145736 | tf_op jit(solution)/shard_map/ppermute | solution.py:427
  46.8 2.6 %collective-permute-done.3.swapped = bf16[512,1024]{1,0:T(8,128)(2,1)S(1)} collective-permute-done((bf16[512,1024]{1,0:T(8,128)(2,1)S(1)}, bf16[512,1024]{1,0:T(8,128)(2,1)S(1)}, u32[]{:S(2)}, u32[]{:S(2)}) %collective-permute-start.3) | collective-permute-done | bytes 1048608 | tf_op jit(solution)/shard_map/ppermute | solution.py:427
  49.4 1.0 copy-done.3
  50.4 5.3 %shard_map.206 = (bf16[512,256]{1,0:T(8,128)(2,1)}, bf16[512,1024]{1,0:T(8,128)(2,1)}) custom-call(s32[1]{0:T(128)} %bitcast.core, bf16[512,1024]{1,0:T(8,128)(2,1)} %bitcast.27, bf16[512,1024]{1,0:T(8,128)(2,1)} %copy-done.3, bf16[2048,256]{1,0:T(8,128)(2,1)} %bitcast.29, bf16[2048,256]{1,0:T(8,128)(2,1)} %bitcast.30, bf16[256,2048]{1,0:T(8,128)(2,1)} %bitcast.24), custom_call_target="tpu_custom_call" | custom-call | tf_op jit(solution)/shard_map/pallas_call | solution.py:322
  55.7 2.0 %collective-permute-start.4 = (bf16[512,1024]{1,0:T(8,128)(2,1)}, bf16[512,1024]{1,0:T(8,128)(2,1)S(1)}, u32[]{:S(2)}, u32[]{:S(2)}) collective-permute-start(bf16[512,1024]{1,0:T(8,128)(2,1)} %get-tuple-element.21), channel_id=1, source_target_pairs={{0,1},{1,0},{2,3},{3,2},{4,5},{5,4},{6,7},{7,6},{8,9},{9,8},{10,11... | collective-permute-start | bytes 3145736 | tf_op jit(solution)/shard_map/ppermute | solution.py:439
  57.7 4.5 %all-to-all-start.2 = ((bf16[8,64,128]{2,1,0:T(8,128)(2,1)}), bf16[8,64,128]{2,1,0:T(8,128)(2,1)S(1)}, u32[]{:S(2)}, u32[]{:S(2)}) async-start(bf16[8,64,128]{2,1,0:T(8,128)(2,1)} %get-tuple-element.23), calls=%async_computation.2 | async-start | bytes 262144 | tf_op jit(solution)/shard_map/all_to_all | solution.py:418
  62.2 0.0 collective-permute-done.4.landed
  62.2 1.0 copy-done.2
  63.1 3.4 %shard_map.207 = bf16[512,1024]{1,0:T(8,128)(2,1)} custom-call(s32[1]{0:T(128)} %bitcast.core, bf16[512,256]{1,0:T(8,128)(2,1)} %get-tuple-element.20.hidden, bf16[512,1024]{1,0:T(8,128)(2,1)} %copy-done.2, bf16[256,2048]{1,0:T(8,128)(2,1)} %bitcast.25), custom_call_target="tpu_custom_call" | custom-call | tf_op jit(solution)/shard_map/pallas_call | solution.py:322
  66.5 5.3 %all-to-all-done.2.arrived = bf16[8,64,128]{2,1,0:T(8,128)(2,1)S(1)} async-done(((bf16[8,64,128]{2,1,0:T(8,128)(2,1)}), bf16[8,64,128]{2,1,0:T(8,128)(2,1)S(1)}, u32[]{:S(2)}, u32[]{:S(2)}) %all-to-all-start.2) | async-done | bytes 131104 | tf_op jit(solution)/shard_map/all_to_all | solution.py:418
  71.8 0.7 copy-done.4
  72.4 6.4 %all-to-all-start.1 = ((bf16[32,16,1024]{2,1,0:T(8,128)(2,1)}), bf16[32,16,1024]{2,1,0:T(8,128)(2,1)S(1)}, u32[]{:S(2)}, u32[]{:S(2)}) async-start(bf16[32,16,1024]{2,1,0:T(8,128)(2,1)} %bitcast.23), calls=%async_computation.1 | async-start | bytes 2097152 | tf_op jit(solution)/shard_map/all_to_all | solution.py:449
  78.8 3.8 %shard_map.208 = (bf16[8,8,2048]{2,1,0:T(8,128)(2,1)}, bf16[8,8,2048]{2,1,0:T(8,128)(2,1)}) custom-call(s32[1]{0:T(128)} %bitcast.7.high.place, s32[1]{0:T(128)} %bitcast.core, bf16[8,64,128]{2,1,0:T(8,128)(2,1)} %copy-done.4, f32[64,128]{1,0:T(8,128)} %get-tuple-element.24.before, f32[64,128]{1,0:T(8,128)} %get-tuple-element.25.after, ...), custom_call_target="tpu_custom_call" | custom-call | tf_op jit(solution)/shard_map/pallas_call | solution.py:322
  82.6 1.9 %collective-permute-start.5 = (bf16[8,8,2048]{2,1,0:T(8,128)(2,1)}, bf16[8,8,2048]{2,1,0:T(8,128)(2,1)S(1)}, u32[]{:S(2)}, u32[]{:S(2)}) collective-permute-start(bf16[8,8,2048]{2,1,0:T(8,128)(2,1)} %get-tuple-element.29), channel_id=1, source_target_pairs={{0,1},{1,0},{2,3},{3,2},{4,5},{5,4},{6,7},{7,6},{8,9},{9,8},{10,11... | collective-permute-start | bytes 786440 | tf_op jit(solution)/shard_map/ppermute | solution.py:466
  84.6 1.7 %collective-permute-done.5.landed = bf16[8,8,2048]{2,1,0:T(8,128)(2,1)S(1)} collective-permute-done((bf16[8,8,2048]{2,1,0:T(8,128)(2,1)}, bf16[8,8,2048]{2,1,0:T(8,128)(2,1)S(1)}, u32[]{:S(2)}, u32[]{:S(2)}) %collective-permute-start.5) | collective-permute-done | bytes 262176 | tf_op jit(solution)/shard_map/ppermute | solution.py:466
  86.3 20.6 %all-to-all-done.1 = bf16[32,16,1024]{2,1,0:T(8,128)(2,1)S(1)} async-done(((bf16[32,16,1024]{2,1,0:T(8,128)(2,1)}), bf16[32,16,1024]{2,1,0:T(8,128)(2,1)S(1)}, u32[]{:S(2)}, u32[]{:S(2)}) %all-to-all-start.1) | async-done | bytes 1048608 | tf_op jit(solution)/shard_map/all_to_all | solution.py:449
  106.9 1.0 copy-done
  107.9 2.6 %shard_map.209 = bf16[8,256,128]{2,1,0:T(8,128)(2,1)} custom-call(bf16[512,1024]{1,0:T(8,128)(2,1)} %bitcast.22, bf16[512,128]{1,0:T(8,128)(2,1)} %get-tuple-element.22.weighing, bf16[8,8,2048]{2,1,0:T(8,128)(2,1)} %get-tuple-element.28.own, bf16[8,8,2048]{2,1,0:T(8,128)(2,1)} %copy-done.5), custom_call_target="tpu_custom_call" | custom-call | tf_op jit(solution)/shard_map/pallas_call | solution.py:322
  110.4 23.2 %all_to_all.20.shares = bf16[8,256,128]{2,1,0:T(8,128)(2,1)} all-to-all(bf16[8,256,128]{2,1,0:T(8,128)(2,1)} %shard_map.209), channel_id=1, replica_groups={{0,2,4,6,8,10,12,14},{1,3,5,7,9,11,13,15},{16,18,20,22,24,26,28,30},{17..., dimensions={0} | all-to-all | bytes 1048576 | tf_op jit(solution)/shard_map/all_to_all | solution.py:477
  133.7 1.7 %shard_map.210 = (bf16[8,2048]{1,0:T(8,128)(2,1)}, bf16[128,128]{1,0:T(8,128)(2,1)}) custom-call(bf16[8,256,128]{2,1,0:T(8,128)(2,1)} %all_to_all.20.shares), custom_call_target="tpu_custom_call" | custom-call | tf_op jit(solution)/shard_map/pallas_call | solution.py:322
  (13 shorter events, 0.0 us)
Async XLA Ops:
  3.4 41.5 %all-to-all-start = ((bf16[32,16,1024]{2,1,0:T(8,128)(2,1)}), bf16[32,16,1024]{2,1,0:T(8,128)(2,1)S(1)}, u32[]{:S(2)}, u32[]{:S(2)}) async-start(bf16[32,16,1024]{2,1,0:T(8,128)(2,1)} %bitcast.28), calls=%async_computation | async-start | bytes 2097152 | tf_op jit(solution)/shard_map/all_to_all | solution.py:377
  27.5 8.6 %collective-permute-start = (bf16[128,128]{1,0:T(8,128)(2,1)}, bf16[128,128]{1,0:T(8,128)(2,1)S(1)}, u32[]{:S(2)}, u32[]{:S(2)}) collective-permute-start(bf16[128,128]{1,0:T(8,128)(2,1)} %get-tuple-element.17.refs_0_), channel_id=1, source_target_pairs={{0,16},{16,32},{32,48},{48,0},{64,80},{80,96},{96,112},{112,64},{1... | collective-permute-start | bytes 98312 | tf_op jit(solution)/shard_map/ppermute | solution.py:401
  30.6 8.0 %collective-permute-start.1 = (bf16[128,128]{1,0:T(8,128)(2,1)}, bf16[128,128]{1,0:T(8,128)(2,1)S(1)}, u32[]{:S(2)}, u32[]{:S(2)}) collective-permute-start(bf16[128,128]{1,0:T(8,128)(2,1)} %get-tuple-element.17.refs_0_), channel_id=1, source_target_pairs={{0,32},{16,48},{32,0},{48,16},{64,96},{80,112},{96,64},{112,80},{1... | collective-permute-start | bytes 98312 | tf_op jit(solution)/shard_map/ppermute | solution.py:401
  33.4 6.2 %collective-permute-start.2 = (bf16[128,128]{1,0:T(8,128)(2,1)}, bf16[128,128]{1,0:T(8,128)(2,1)S(1)}, u32[]{:S(2)}, u32[]{:S(2)}) collective-permute-start(bf16[128,128]{1,0:T(8,128)(2,1)} %get-tuple-element.17.refs_0_), channel_id=1, source_target_pairs={{0,48},{16,0},{32,16},{48,32},{64,112},{80,64},{96,80},{112,96},{1... | collective-permute-start | bytes 98312 | tf_op jit(solution)/shard_map/ppermute | solution.py:401
  36.2 3.4 %copy-start.6 = (bf16[128,128]{1,0:T(8,128)(2,1)}, bf16[128,128]{1,0:T(8,128)(2,1)S(1)}, u32[]{:S(2)}) copy-start(bf16[128,128]{1,0:T(8,128)(2,1)S(1)} %collective-permute-done.refs_1_) | copy-start | bytes 98308
  38.6 0.9 copy-start.7
  39.5 0.6 copy-start.8
  44.9 4.5 %copy-start.1 = (bf16[32,16,1024]{2,1,0:T(8,128)(2,1)}, bf16[32,16,1024]{2,1,0:T(8,128)(2,1)S(1)}, u32[]{:S(2)}) copy-start(bf16[32,16,1024]{2,1,0:T(8,128)(2,1)S(1)} %all-to-all-done) | copy-start | bytes 3145732
  44.9 4.5 %collective-permute-start.3 = (bf16[512,1024]{1,0:T(8,128)(2,1)S(1)}, bf16[512,1024]{1,0:T(8,128)(2,1)S(1)}, u32[]{:S(2)}, u32[]{:S(2)}) collective-permute-start(bf16[512,1024]{1,0:T(8,128)(2,1)S(1)} %bitcast.26), channel_id=1, source_target_pairs={{0,1},{1,0},{2,3},{3,2},{4,5},{5,4},{6,7},{7,6},{8,9},{9,8},{10,11... | collective-permute-start | bytes 3145736 | tf_op jit(solution)/shard_map/ppermute | solution.py:427
  49.4 1.0 copy-start.3
  55.7 6.5 %collective-permute-start.4 = (bf16[512,1024]{1,0:T(8,128)(2,1)}, bf16[512,1024]{1,0:T(8,128)(2,1)S(1)}, u32[]{:S(2)}, u32[]{:S(2)}) collective-permute-start(bf16[512,1024]{1,0:T(8,128)(2,1)} %get-tuple-element.21), channel_id=1, source_target_pairs={{0,1},{1,0},{2,3},{3,2},{4,5},{5,4},{6,7},{7,6},{8,9},{9,8},{10,11... | collective-permute-start | bytes 3145736 | tf_op jit(solution)/shard_map/ppermute | solution.py:439
  57.7 14.1 %all-to-all-start.2 = ((bf16[8,64,128]{2,1,0:T(8,128)(2,1)}), bf16[8,64,128]{2,1,0:T(8,128)(2,1)S(1)}, u32[]{:S(2)}, u32[]{:S(2)}) async-start(bf16[8,64,128]{2,1,0:T(8,128)(2,1)} %get-tuple-element.23), calls=%async_computation.2 | async-start | bytes 262144 | tf_op jit(solution)/shard_map/all_to_all | solution.py:418
  62.2 1.0 copy-start.2
  71.8 0.7 copy-start.4
  72.4 34.4 %all-to-all-start.1 = ((bf16[32,16,1024]{2,1,0:T(8,128)(2,1)}), bf16[32,16,1024]{2,1,0:T(8,128)(2,1)S(1)}, u32[]{:S(2)}, u32[]{:S(2)}) async-start(bf16[32,16,1024]{2,1,0:T(8,128)(2,1)} %bitcast.23), calls=%async_computation.1 | async-start | bytes 2097152 | tf_op jit(solution)/shard_map/all_to_all | solution.py:449
  82.6 3.6 %collective-permute-start.5 = (bf16[8,8,2048]{2,1,0:T(8,128)(2,1)}, bf16[8,8,2048]{2,1,0:T(8,128)(2,1)S(1)}, u32[]{:S(2)}, u32[]{:S(2)}) collective-permute-start(bf16[8,8,2048]{2,1,0:T(8,128)(2,1)} %get-tuple-element.29), channel_id=1, source_target_pairs={{0,1},{1,0},{2,3},{3,2},{4,5},{5,4},{6,7},{7,6},{8,9},{9,8},{10,11... | collective-permute-start | bytes 786440 | tf_op jit(solution)/shard_map/ppermute | solution.py:466
  86.3 20.6 %copy-start.5 = (bf16[8,8,2048]{2,1,0:T(8,128)(2,1)}, bf16[8,8,2048]{2,1,0:T(8,128)(2,1)S(1)}, u32[]{:S(2)}) copy-start(bf16[8,8,2048]{2,1,0:T(8,128)(2,1)S(1)} %collective-permute-done.5.landed) | copy-start | bytes 786436
  106.9 1.0 copy-start

commit v2 on v1

--- a/solution.py
+++ b/solution.py
@@ -14,6 +14,7 @@
 F32 = jnp.float32
 BF16 = jnp.bfloat16
 ROW = 4
+LIMIT = 24 * 1024 * 1024
 
 
 def mm(a, b, precision=HIGH):
@@ -316,6 +317,16 @@
     buffer[...] = mm(placing, mine.astype(BF16), None).astype(BF16)
 
 
+def placed(value, space):
+    if isinstance(value, jax.ShapeDtypeStruct):
+        return space(value.shape, value.dtype)
+    return pltpu.with_memory_space_constraint(value, space)
+
+
+near = lambda value: placed(value, pltpu.VMEM)
+far = lambda value: placed(value, pltpu.HBM)
+
+
 def call(kernel, outs, scalars, *args):
     smem = pl.BlockSpec(memory_space=pltpu.SMEM)
     vmem = pl.BlockSpec(memory_space=pltpu.VMEM)
@@ -324,6 +335,7 @@
         out_shape=outs,
         in_specs=[smem] * len(scalars) + [vmem] * len(args),
         out_specs=jax.tree.map(lambda _: vmem, outs),
+        compiler_params=pltpu.CompilerParams(vmem_limit_bytes=LIMIT),
     )(*scalars, *args)
 
 
@@ -367,34 +379,34 @@
 
     buffer, weighing = call(
         functools.partial(dispatch_kernel, experts, slots),
-        (shape((experts * slots, half), BF16), shape((experts * slots, tokens), BF16)),
+        (shape((experts * slots, half), BF16), far(shape((experts * slots, tokens), BF16))),
         (scalar(core),),
-        moe_rows,
-        moe_gain.reshape(1, -1),
-        routes.T,
-        route_weight.T,
+        far(moe_rows),
+        far(moe_gain.reshape(1, -1)),
+        far(routes.T),
+        far(route_weight.T),
     )
     arrived = lax.all_to_all(
         buffer.reshape(experts, slots, half), "ep", split_axis=0, concat_axis=0, tiled=True
     ).reshape(experts * slots, half)
 
-    reads = shape((tokens, 2 * width), F32)
-    wide = shape((width, 2 * width), F32)
+    reads = far(shape((tokens, 2 * width), F32))
+    wide = far(shape((width, 2 * width), F32))
     reads_f, reads_b, both = call(
         mixer_kernel,
-        (reads, reads, shape((2 * width, 2 * width), BF16)),
+        (reads, reads, near(shape((2 * width, 2 * width), BF16))),
         (),
-        mixer_input_rows,
-        mix_gain.reshape(1, -1),
-        w_recept.T,
-        w_key.T,
-        w_value.T,
-        lowered_map_factor.T,
-        decay_up,
-        rate_up,
-        decay_base.reshape(1, -1),
-        rate_base.reshape(1, -1),
-        decay_shift.T,
+        far(mixer_input_rows),
+        far(mix_gain.reshape(1, -1)),
+        far(w_recept.T),
+        far(w_key.T),
+        far(w_value.T),
+        far(lowered_map_factor.T),
+        far(decay_up),
+        far(rate_up),
+        far(decay_base.reshape(1, -1)),
+        far(rate_base.reshape(1, -1)),
+        far(decay_shift.T),
     )
 
     others = [
@@ -407,10 +419,10 @@
     ]
     sent, before, after = call(
         row_kernel,
-        (shape((rows, width, 2 * width), BF16), wide, wide),
+        (near(shape((rows, width, 2 * width), BF16)), wide, wide),
         (scalar(low), scalar(high)),
-        both,
-        *others,
+        near(both),
+        *[near(other) for other in others],
     )
 
     arrived, sent = lax.optimization_barrier((arrived, sent))
@@ -428,22 +440,22 @@
     inner = exp_gate.shape[2]
     hidden, away = call(
         functools.partial(expert_kernel, piece),
-        (shape((experts * slots, inner), BF16), shape((experts * slots, half), BF16)),
+        (near(shape((experts * slots, inner), BF16)), near(shape((experts * slots, half), BF16))),
         (scalar(core),),
-        arrived,
-        swapped,
-        exp_gate[0],
-        exp_up[0],
-        exp_down[0],
+        near(arrived),
+        near(swapped),
+        far(exp_gate[0]),
+        near(exp_up[0]),
+        near(exp_down[0]),
     )
     landed = lax.ppermute(away, "tp", swap)
     paired = call(
         functools.partial(pair_kernel, piece),
-        shape((experts * slots, half), BF16),
+        near(shape((experts * slots, half), BF16)),
         (scalar(core),),
-        hidden,
-        landed,
-        exp_down[0],
+        near(hidden),
+        near(landed),
+        near(exp_down[0]),
     )
 
     returned = lax.all_to_all(
@@ -453,26 +465,26 @@
     shares = shape((chips, tokens // tp, model), BF16)
     own_rows, away_rows = call(
         output_kernel,
-        (shares, shares),
+        (near(shares), near(shares)),
         (scalar(high), scalar(core)),
-        carried,
-        before,
-        after,
-        reads_f,
-        reads_b,
-        out_gain.reshape(1, -1),
-        w_output,
+        near(carried),
+        far(before),
+        far(after),
+        far(reads_f),
+        far(reads_b),
+        far(out_gain.reshape(1, -1)),
+        far(w_output),
     )
     landed_rows = lax.ppermute(away_rows, "tp", swap)
 
     parts = call(
         combine_kernel,
-        shape((chips, 2 * tokens, piece), BF16),
+        near(shape((chips, 2 * tokens, piece), BF16)),
         (),
-        returned,
-        weighing,
-        own_rows,
-        landed_rows,
+        near(returned),
+        far(weighing),
+        near(own_rows),
+        near(landed_rows),
     )
     parts = lax.all_to_all(
         parts,
@@ -486,7 +498,7 @@
         finish_kernel,
         (shape((tokens // tp, model), BF16), shape((tokens, piece), BF16)),
         (),
-        parts,
+        near(parts),
     )
     return (mix_out, moe_out)
 

time: 136 us -> 127 us (0.934)
  the two profiles are of different devices: /device:TPU:4 before, /device:TPU:6 now
where the time goes in v2:
time: 127 us
  waiting for transfers between devices  40.5 us (32%)
  starting transfers between devices  37.2 us (29%)
  Pallas kernels  25.6 us (20%)
  blocking collectives  22.7 us (18%)
    pallas_call x8, Pallas kernels, call(): pl.pallas_call(kernel, out_shape=outs, in_specs=[smem] * len(scalars) + [...  25.6 us
    all_to_all x1, blocking collectives, shards(): lax.all_to_all(parts, 'tp', split_axis=0, concat_axis=0, tiled=True, axis...  22.7 us
    all_to_all x1, waiting for transfers between devices, shards(): lax.all_to_all(paired.reshape(experts, slots, half), 'ep', split_axis=0,...  21.2 us
    all_to_all x1, starting transfers between devices, shards(): lax.all_to_all(buffer.reshape(experts, slots, half), 'ep', split_axis=0,...  13.5 us
    ppermute x3, starting transfers between devices, shards(): lax.ppermute(both, 'ep', [(k, k // across * across + (k + m) % across) fo...  8.65 us
    all_to_all x1, waiting for transfers between devices, shards(): lax.all_to_all(sent, 'ep', split_axis=0, concat_axis=0, tiled=True, axis_...  7.88 us
    ppermute x3, waiting for transfers between devices, shards(): lax.ppermute(both, 'ep', [(k, k // across * across + (k + m) % across) fo...  5.21 us
    all_to_all x1, starting transfers between devices, shards(): lax.all_to_all(paired.reshape(experts, slots, half), 'ep', split_axis=0,...  4.67 us
  transfers between devices with their start and end apart: 9, of which 7 were waited for; matrix products, arithmetic and copies ran while one was open for 0% of the time, Pallas kernels for 13%

profile of v2, /device:TPU:6, one launch (start us, length us, event | category | flops | bytes accessed | tf_op | source)
XLA Modules:
  0.0 126.7 jit_solution(13835029097110717328)
XLA Ops:
  0.6 2.7 %shard_map.203 = (bf16[512,1024]{1,0:T(8,128)(2,1)}, bf16[512,128]{1,0:T(8,128)(2,1)}) custom-call(s32[1]{0:T(128)} %bitcast.core, bf16[128,2048]{1,0:T(8,128)(2,1)} %rows.1, f32[1,2048]{1,0:T(1,128)} %bitcast.33, s32[2,128]{1,0:T(2,128)} %bitcast.35, f32[2,128]{1,0:T(2,128)} %bitcast.36), custom_call_target="tpu_custom_call" | custom-call | tf_op jit(solution)/shard_map/pallas_call | solution.py:333
  3.3 0.0 copy-start.1
  3.3 13.5 %all-to-all-start = ((bf16[32,16,1024]{2,1,0:T(8,128)(2,1)}), bf16[32,16,1024]{2,1,0:T(8,128)(2,1)S(1)}, u32[]{:S(2)}, u32[]{:S(2)}) async-start(bf16[32,16,1024]{2,1,0:T(8,128)(2,1)} %bitcast.4), calls=%async_computation | async-start | bytes 2097152 | tf_op jit(solution)/shard_map/all_to_all | solution.py:389
  16.9 0.0 copy-start
  16.9 10.7 %shard_map.204 = (f32[128,128]{1,0:T(8,128)}, f32[128,128]{1,0:T(8,128)}, bf16[128,128]{1,0:T(8,128)(2,1)S(1)}) custom-call(bf16[128,2048]{1,0:T(8,128)(2,1)} %refs_0_.1, f32[1,2048]{1,0:T(1,128)} %bitcast.34, bf16[64,2048]{1,0:T(8,128)(2,1)} %bitcast.29, bf16[64,2048]{1,0:T(8,128)(2,1)} %bitcast.30, bf16[64,2048]{1,0:T(8,128)(2,1)} %bitcast.31, ...), custom_call_target="tpu_custom_call" | custom-call | tf_op jit(solution)/shard_map/pallas_call | solution.py:333
  27.6 2.1 %collective-permute-start = (bf16[128,128]{1,0:T(8,128)(2,1)S(1)}, bf16[128,128]{1,0:T(8,128)(2,1)S(1)}, u32[]{:S(2)}, u32[]{:S(2)}) collective-permute-start(bf16[128,128]{1,0:T(8,128)(2,1)S(1)} %get-tuple-element.17.refs_0_), channel_id=1, source_target_pairs={{0,16},{16,32},{32,48},{48,0},{64,80},{80,96},{96,112},{112,64},{1... | collective-permute-start | bytes 98312 | tf_op jit(solution)/shard_map/ppermute | solution.py:413
  29.8 4.6 %collective-permute-start.1 = (bf16[128,128]{1,0:T(8,128)(2,1)S(1)}, bf16[128,128]{1,0:T(8,128)(2,1)S(1)}, u32[]{:S(2)}, u32[]{:S(2)}) collective-permute-start(bf16[128,128]{1,0:T(8,128)(2,1)S(1)} %get-tuple-element.17.refs_0_), channel_id=1, source_target_pairs={{0,32},{16,48},{32,0},{48,16},{64,96},{80,112},{96,64},{112,80},{1... | collective-permute-start | bytes 98312 | tf_op jit(solution)/shard_map/ppermute | solution.py:413
  34.4 1.9 %collective-permute-start.2 = (bf16[128,128]{1,0:T(8,128)(2,1)S(1)}, bf16[128,128]{1,0:T(8,128)(2,1)S(1)}, u32[]{:S(2)}, u32[]{:S(2)}) collective-permute-start(bf16[128,128]{1,0:T(8,128)(2,1)S(1)} %get-tuple-element.17.refs_0_), channel_id=1, source_target_pairs={{0,48},{16,0},{32,16},{48,32},{64,112},{80,64},{96,80},{112,96},{1... | collective-permute-start | bytes 98312 | tf_op jit(solution)/shard_map/ppermute | solution.py:413
  36.3 0.0 collective-permute-done.refs_1_
  36.3 1.8 %collective-permute-done.1.refs_2_ = bf16[128,128]{1,0:T(8,128)(2,1)S(1)} collective-permute-done((bf16[128,128]{1,0:T(8,128)(2,1)S(1)}, bf16[128,128]{1,0:T(8,128)(2,1)S(1)}, u32[]{:S(2)}, u32[]{:S(2)}) %collective-permute-start.1) | collective-permute-done | bytes 32800 | tf_op jit(solution)/shard_map/ppermute | solution.py:413
  38.1 3.4 %collective-permute-done.2.refs_3_ = bf16[128,128]{1,0:T(8,128)(2,1)S(1)} collective-permute-done((bf16[128,128]{1,0:T(8,128)(2,1)S(1)}, bf16[128,128]{1,0:T(8,128)(2,1)S(1)}, u32[]{:S(2)}, u32[]{:S(2)}) %collective-permute-start.2) | collective-permute-done | bytes 32800 | tf_op jit(solution)/shard_map/ppermute | solution.py:413
  41.5 1.4 %shard_map.205 = (bf16[8,64,128]{2,1,0:T(8,128)(2,1)}, f32[64,128]{1,0:T(8,128)}, f32[64,128]{1,0:T(8,128)}) custom-call(s32[1]{0:T(128)} %bitcast.6.place, s32[1]{0:T(128)} %bitcast.7.high.place, bf16[128,128]{1,0:T(8,128)(2,1)S(1)} %get-tuple-element.17.refs_0_, bf16[128,128]{1,0:T(8,128)(2,1)S(1)} %collective-permute-done.refs_1_, ...), custom_call_target="tpu_custom_call" | custom-call | tf_op jit(solution)/shard_map/pallas_call | solution.py:333
  42.9 2.0 %all-to-all-done = bf16[32,16,1024]{2,1,0:T(8,128)(2,1)S(1)} async-done(((bf16[32,16,1024]{2,1,0:T(8,128)(2,1)}), bf16[32,16,1024]{2,1,0:T(8,128)(2,1)S(1)}, u32[]{:S(2)}, u32[]{:S(2)}) %all-to-all-start) | async-done | bytes 1048608 | tf_op jit(solution)/shard_map/all_to_all | solution.py:389
  45.0 1.9 %collective-permute-start.3 = (bf16[512,1024]{1,0:T(8,128)(2,1)S(1)}, bf16[512,1024]{1,0:T(8,128)(2,1)S(1)}, u32[]{:S(2)}, u32[]{:S(2)}) collective-permute-start(bf16[512,1024]{1,0:T(8,128)(2,1)S(1)} %bitcast.25), channel_id=1, source_target_pairs={{0,1},{1,0},{2,3},{3,2},{4,5},{5,4},{6,7},{7,6},{8,9},{9,8},{10,11... | collective-permute-start | bytes 3145736 | tf_op jit(solution)/shard_map/ppermute | solution.py:439
  46.9 2.6 %collective-permute-done.3.swapped = bf16[512,1024]{1,0:T(8,128)(2,1)S(1)} collective-permute-done((bf16[512,1024]{1,0:T(8,128)(2,1)S(1)}, bf16[512,1024]{1,0:T(8,128)(2,1)S(1)}, u32[]{:S(2)}, u32[]{:S(2)}) %collective-permute-start.3) | collective-permute-done | bytes 1048608 | tf_op jit(solution)/shard_map/ppermute | solution.py:439
  49.5 0.0 copy-done.1
  49.5 0.0 copy-done
  49.5 4.0 %shard_map.206 = (bf16[512,256]{1,0:T(8,128)(2,1)S(1)}, bf16[512,1024]{1,0:T(8,128)(2,1)}) custom-call(s32[1]{0:T(128)} %bitcast.core, bf16[512,1024]{1,0:T(8,128)(2,1)S(1)} %bitcast.26, bf16[512,1024]{1,0:T(8,128)(2,1)S(1)} %collective-permute-done.3.swapped, bf16[2048,256]{1,0:T(8,128)(2,1)} %bitcast.28, bf16[2048,256]{1,0:T(8,128)(2,1)S(1)} %bitcast.27, ...), custom_call_target="tpu_custom_call" | custom-call | tf_op jit(solution)/shard_map/pallas_call | solution.py:333
  53.5 2.0 %collective-permute-start.4 = (bf16[512,1024]{1,0:T(8,128)(2,1)}, bf16[512,1024]{1,0:T(8,128)(2,1)S(1)}, u32[]{:S(2)}, u32[]{:S(2)}) collective-permute-start(bf16[512,1024]{1,0:T(8,128)(2,1)} %get-tuple-element.21), channel_id=1, source_target_pairs={{0,1},{1,0},{2,3},{3,2},{4,5},{5,4},{6,7},{7,6},{8,9},{9,8},{10,11... | collective-permute-start | bytes 3145736 | tf_op jit(solution)/shard_map/ppermute | solution.py:451
  55.6 4.5 %all-to-all-start.2 = ((bf16[8,64,128]{2,1,0:T(8,128)(2,1)}), bf16[8,64,128]{2,1,0:T(8,128)(2,1)S(1)}, u32[]{:S(2)}, u32[]{:S(2)}) async-start(bf16[8,64,128]{2,1,0:T(8,128)(2,1)} %get-tuple-element.23), calls=%async_computation.2 | async-start | bytes 262144 | tf_op jit(solution)/shard_map/all_to_all | solution.py:430
  60.0 0.0 collective-permute-done.4.landed
  60.0 1.7 %shard_map.207 = bf16[512,1024]{1,0:T(8,128)(2,1)} custom-call(s32[1]{0:T(128)} %bitcast.core, bf16[512,256]{1,0:T(8,128)(2,1)S(1)} %get-tuple-element.20.hidden, bf16[512,1024]{1,0:T(8,128)(2,1)S(1)} %collective-permute-done.4.landed, bf16[256,2048]{1,0:T(8,128)(2,1)S(1)} %bitcast.24), custom_call_target="tpu_custom_call" | custom-call | tf_op jit(solution)/shard_map/pallas_call | solution.py:333
  61.7 7.9 %all-to-all-done.2.arrived = bf16[8,64,128]{2,1,0:T(8,128)(2,1)S(1)} async-done(((bf16[8,64,128]{2,1,0:T(8,128)(2,1)}), bf16[8,64,128]{2,1,0:T(8,128)(2,1)S(1)}, u32[]{:S(2)}, u32[]{:S(2)}) %all-to-all-start.2) | async-done | bytes 131104 | tf_op jit(solution)/shard_map/all_to_all | solution.py:430
  69.6 4.7 %all-to-all-start.1 = ((bf16[32,16,1024]{2,1,0:T(8,128)(2,1)}), bf16[32,16,1024]{2,1,0:T(8,128)(2,1)S(1)}, u32[]{:S(2)}, u32[]{:S(2)}) async-start(bf16[32,16,1024]{2,1,0:T(8,128)(2,1)} %bitcast.19), calls=%async_computation.1 | async-start | bytes 2097152 | tf_op jit(solution)/shard_map/all_to_all | solution.py:461
  74.3 3.1 %shard_map.208 = (bf16[8,8,2048]{2,1,0:T(8,128)(2,1)S(1)}, bf16[8,8,2048]{2,1,0:T(8,128)(2,1)S(1)}) custom-call(s32[1]{0:T(128)} %bitcast.7.high.place, s32[1]{0:T(128)} %bitcast.core, bf16[8,64,128]{2,1,0:T(8,128)(2,1)S(1)} %all-to-all-done.2.arrived, f32[64,128]{1,0:T(8,128)} %get-tuple-element.24.before, f32[64,128]{1,0:T(8,128)} %get-tuple-element.25.after, ...), custom_call_target="tpu_custom_call" | custom-call | tf_op jit(solution)/shard_map/pallas_call | solution.py:333
  77.4 1.9 %collective-permute-start.5 = (bf16[8,8,2048]{2,1,0:T(8,128)(2,1)S(1)}, bf16[8,8,2048]{2,1,0:T(8,128)(2,1)S(1)}, u32[]{:S(2)}, u32[]{:S(2)}) collective-permute-start(bf16[8,8,2048]{2,1,0:T(8,128)(2,1)S(1)} %get-tuple-element.29), channel_id=1, source_target_pairs={{0,1},{1,0},{2,3},{3,2},{4,5},{5,4},{6,7},{7,6},{8,9},{9,8},{10,11... | collective-permute-start | bytes 786440 | tf_op jit(solution)/shard_map/ppermute | solution.py:478
  79.3 1.5 %collective-permute-done.5.landed = bf16[8,8,2048]{2,1,0:T(8,128)(2,1)S(1)} collective-permute-done((bf16[8,8,2048]{2,1,0:T(8,128)(2,1)S(1)}, bf16[8,8,2048]{2,1,0:T(8,128)(2,1)S(1)}, u32[]{:S(2)}, u32[]{:S(2)}) %collective-permute-start.5) | collective-permute-done | bytes 262176 | tf_op jit(solution)/shard_map/ppermute | solution.py:478
  80.8 21.2 %all-to-all-done.1 = bf16[32,16,1024]{2,1,0:T(8,128)(2,1)S(1)} async-done(((bf16[32,16,1024]{2,1,0:T(8,128)(2,1)}), bf16[32,16,1024]{2,1,0:T(8,128)(2,1)S(1)}, u32[]{:S(2)}, u32[]{:S(2)}) %all-to-all-start.1) | async-done | bytes 1048608 | tf_op jit(solution)/shard_map/all_to_all | solution.py:461
  102.0 1.3 %shard_map.209 = bf16[8,256,128]{2,1,0:T(8,128)(2,1)S(1)} custom-call(bf16[512,1024]{1,0:T(8,128)(2,1)S(1)} %bitcast.22, bf16[512,128]{1,0:T(8,128)(2,1)} %get-tuple-element.22.weighing, bf16[8,8,2048]{2,1,0:T(8,128)(2,1)S(1)} %get-tuple-element.28.own, bf16[8,8,2048]{2,1,0:T(8,128)(2,1)S(1)} %collective-permute-done.5.landed), custom_call_target="tpu_custom_call" | custom-call | tf_op jit(solution)/shard_map/pallas_call | solution.py:333
  103.3 22.7 %all_to_all.20.shares = bf16[8,256,128]{2,1,0:T(8,128)(2,1)S(1)} all-to-all(bf16[8,256,128]{2,1,0:T(8,128)(2,1)S(1)} %shard_map.209), channel_id=1, replica_groups={{0,2,4,6,8,10,12,14},{1,3,5,7,9,11,13,15},{16,18,20,22,24,26,28,30},{17..., dimensions={0} | all-to-all | bytes 1048576 | tf_op jit(solution)/shard_map/all_to_all | solution.py:489
  126.0 0.7 shard_map.210
Async XLA Ops:
  3.3 46.2 %copy-start.1 = (bf16[1,2048,256]{2,1,0:T(8,128)(2,1)S(1)}, bf16[1,2048,256]{2,1,0:T(8,128)(2,1)}, u32[]{:S(2)}) copy-start(bf16[1,2048,256]{2,1,0:T(8,128)(2,1)} %param.38) | copy-start | bytes 3145732
  3.3 41.6 %all-to-all-start = ((bf16[32,16,1024]{2,1,0:T(8,128)(2,1)}), bf16[32,16,1024]{2,1,0:T(8,128)(2,1)S(1)}, u32[]{:S(2)}, u32[]{:S(2)}) async-start(bf16[32,16,1024]{2,1,0:T(8,128)(2,1)} %bitcast.4), calls=%async_computation | async-start | bytes 2097152 | tf_op jit(solution)/shard_map/all_to_all | solution.py:389
  16.9 32.6 %copy-start = (bf16[1,256,2048]{2,1,0:T(8,128)(2,1)S(1)}, bf16[1,256,2048]{2,1,0:T(8,128)(2,1)}, u32[]{:S(2)}) copy-start(bf16[1,256,2048]{2,1,0:T(8,128)(2,1)} %param.39) | copy-start | bytes 3145732
  27.6 8.7 %collective-permute-start = (bf16[128,128]{1,0:T(8,128)(2,1)S(1)}, bf16[128,128]{1,0:T(8,128)(2,1)S(1)}, u32[]{:S(2)}, u32[]{:S(2)}) collective-permute-start(bf16[128,128]{1,0:T(8,128)(2,1)S(1)} %get-tuple-element.17.refs_0_), channel_id=1, source_target_pairs={{0,16},{16,32},{32,48},{48,0},{64,80},{80,96},{96,112},{112,64},{1... | collective-permute-start | bytes 98312 | tf_op jit(solution)/shard_map/ppermute | solution.py:413
  29.8 8.4 %collective-permute-start.1 = (bf16[128,128]{1,0:T(8,128)(2,1)S(1)}, bf16[128,128]{1,0:T(8,128)(2,1)S(1)}, u32[]{:S(2)}, u32[]{:S(2)}) collective-permute-start(bf16[128,128]{1,0:T(8,128)(2,1)S(1)} %get-tuple-element.17.refs_0_), channel_id=1, source_target_pairs={{0,32},{16,48},{32,0},{48,16},{64,96},{80,112},{96,64},{112,80},{1... | collective-permute-start | bytes 98312 | tf_op jit(solution)/shard_map/ppermute | solution.py:413
  34.4 7.2 %collective-permute-start.2 = (bf16[128,128]{1,0:T(8,128)(2,1)S(1)}, bf16[128,128]{1,0:T(8,128)(2,1)S(1)}, u32[]{:S(2)}, u32[]{:S(2)}) collective-permute-start(bf16[128,128]{1,0:T(8,128)(2,1)S(1)} %get-tuple-element.17.refs_0_), channel_id=1, source_target_pairs={{0,48},{16,0},{32,16},{48,32},{64,112},{80,64},{96,80},{112,96},{1... | collective-permute-start | bytes 98312 | tf_op jit(solution)/shard_map/ppermute | solution.py:413
  45.0 4.5 %collective-permute-start.3 = (bf16[512,1024]{1,0:T(8,128)(2,1)S(1)}, bf16[512,1024]{1,0:T(8,128)(2,1)S(1)}, u32[]{:S(2)}, u32[]{:S(2)}) collective-permute-start(bf16[512,1024]{1,0:T(8,128)(2,1)S(1)} %bitcast.25), channel_id=1, source_target_pairs={{0,1},{1,0},{2,3},{3,2},{4,5},{5,4},{6,7},{7,6},{8,9},{9,8},{10,11... | collective-permute-start | bytes 3145736 | tf_op jit(solution)/shard_map/ppermute | solution.py:439
  53.5 6.5 %collective-permute-start.4 = (bf16[512,1024]{1,0:T(8,128)(2,1)}, bf16[512,1024]{1,0:T(8,128)(2,1)S(1)}, u32[]{:S(2)}, u32[]{:S(2)}) collective-permute-start(bf16[512,1024]{1,0:T(8,128)(2,1)} %get-tuple-element.21), channel_id=1, source_target_pairs={{0,1},{1,0},{2,3},{3,2},{4,5},{5,4},{6,7},{7,6},{8,9},{9,8},{10,11... | collective-permute-start | bytes 3145736 | tf_op jit(solution)/shard_map/ppermute | solution.py:451
  55.6 14.1 %all-to-all-start.2 = ((bf16[8,64,128]{2,1,0:T(8,128)(2,1)}), bf16[8,64,128]{2,1,0:T(8,128)(2,1)S(1)}, u32[]{:S(2)}, u32[]{:S(2)}) async-start(bf16[8,64,128]{2,1,0:T(8,128)(2,1)} %get-tuple-element.23), calls=%async_computation.2 | async-start | bytes 262144 | tf_op jit(solution)/shard_map/all_to_all | solution.py:430
  69.6 32.4 %all-to-all-start.1 = ((bf16[32,16,1024]{2,1,0:T(8,128)(2,1)}), bf16[32,16,1024]{2,1,0:T(8,128)(2,1)S(1)}, u32[]{:S(2)}, u32[]{:S(2)}) async-start(bf16[32,16,1024]{2,1,0:T(8,128)(2,1)} %bitcast.19), calls=%async_computation.1 | async-start | bytes 2097152 | tf_op jit(solution)/shard_map/all_to_all | solution.py:461
  77.4 3.4 %collective-permute-start.5 = (bf16[8,8,2048]{2,1,0:T(8,128)(2,1)S(1)}, bf16[8,8,2048]{2,1,0:T(8,128)(2,1)S(1)}, u32[]{:S(2)}, u32[]{:S(2)}) collective-permute-start(bf16[8,8,2048]{2,1,0:T(8,128)(2,1)S(1)} %get-tuple-element.29), channel_id=1, source_target_pairs={{0,1},{1,0},{2,3},{3,2},{4,5},{5,4},{6,7},{7,6},{8,9},{9,8},{10,11... | collective-permute-start | bytes 786440 | tf_op jit(solution)/shard_map/ppermute | solution.py:478

commit v3 on v2

--- a/solution.py
+++ b/solution.py
@@ -10,11 +10,11 @@
 
 
 DECAY_SCALE = math.exp(-0.5)
-HIGH = lax.Precision.HIGHEST
+HIGH = lax.Precision.HIGH
 F32 = jnp.float32
 BF16 = jnp.bfloat16
-ROW = 4
-LIMIT = 24 * 1024 * 1024
+BLOCK = 256
+LIMIT = 16 * 1024 * 1024
 
 
 def mm(a, b, precision=HIGH):
@@ -170,98 +170,86 @@
     return jnp.where(use, maps.astype(F32), plain).astype(BF16)
 
 
-def row_values(place, gathered):
-    count = len(gathered)
-    plain = plain_like(gathered[0][0])
-    ahead, back = ([g[0] for g in gathered], [g[1] for g in gathered])
-    before = chained([kept(ahead[k], k < place, plain) for k in range(count)], False)
-    after = chained([kept(back[k], k > place, plain) for k in range(count)], True)
-    return chained(ahead, False), chained(back, True), before, after
-
-
-def row_kernel(place, high, *refs):
-    held, (sent, before, after) = refs[:-3], refs[-3:]
+def composed(late, early):
+    return mm(late.astype(BF16), with_identity(early.astype(BF16)), None)
+
+
+def joined(high, mine, theirs, before, after):
     width = before.shape[0]
-    count = len(held)
-    held = [(r[:width], r[width:]) for r in held]
-    at = place[0]
-    gathered = []
-    for k in range(count):
-        far = lax.rem(at - k + count, count)
-        chosen = []
-        for side in range(2):
-            value = held[0][side].astype(F32)
-            for m in range(1, count):
-                value = jnp.where(far == m, held[m][side].astype(F32), value)
-            chosen.append(value.astype(BF16))
-        gathered.append(chosen)
-    total_f, total_b, before[...], after[...] = row_values(at, gathered)
+    r = lax.broadcasted_iota(jnp.int32, before.shape, 0)
+    c = lax.broadcasted_iota(jnp.int32, before.shape, 1)
+    plain = (r == c).astype(F32)
+    mine_f, mine_b = (mine[:width].astype(F32), mine[width:].astype(F32))
+    their_f, their_b = (theirs[:width].astype(F32), theirs[width:].astype(F32))
+    before = composed(before, jnp.where(high, their_f, plain))
+    after = composed(after, jnp.where(high, plain, their_b))
+    ahead = composed(jnp.where(high, mine_f, their_f), jnp.where(high, their_f, mine_f))
+    back = composed(jnp.where(high, their_b, mine_b), jnp.where(high, mine_b, their_b))
+    return ahead, back, before, after
+
+
+def first_kernel(high, mine, theirs, total, before, after):
+    width = before.shape[0]
+    r = lax.broadcasted_iota(jnp.int32, before.shape, 0)
+    c = lax.broadcasted_iota(jnp.int32, before.shape, 1)
+    plain = (r == c).astype(F32)
+    ahead, back, before[...], after[...] = joined(high[0] != 0, mine[...], theirs[...], plain, plain)
+    total[:width] = ahead.astype(BF16)
+    total[width:] = back.astype(BF16)
+
+
+def send_kernel(high, run, mine, theirs, before_in, after_in, sent, before, after):
+    ahead, back, before[...], after[...] = joined(
+        high[0] != 0, mine[...], theirs[...], before_in[...], after_in[...]
+    )
     for k in range(sent.shape[0]):
-        sent[k] = jnp.where(k > high[0], total_f, total_b).astype(BF16)
-
-
-def output_values(place, core, arrived, before, after, reads_f, reads_b, gain, w_output, chips):
-    count, width = len(arrived), before.shape[0]
+        sent[k] = jnp.where(k > run[0], ahead, back).astype(BF16)
+
+
+def output_kernel(
+    run, core, arrived, before, after, reads_f, reads_b, gain, w_output, own, away
+):
+    count, width = arrived.shape[0], before.shape[0]
     plain = plain_like(arrived[0])
-    ahead = chained([kept(arrived[k], k < place, plain) for k in range(count)], False)
-    back = chained([kept(arrived[k], k > place, plain) for k in range(count)], True)
-    ahead = mm(before, with_identity(ahead))
-    back = mm(after, with_identity(back))
-    mixed = mm(reads_f, with_identity(ahead)) + mm(reads_b, with_identity(back))
+    ahead = chained([kept(arrived[k], k < run[0], plain) for k in range(count)], False)
+    back = chained([kept(arrived[k], k > run[0], plain) for k in range(count)], True)
+    ahead = mm(before[...], with_identity(ahead))
+    back = mm(after[...], with_identity(back))
+    mixed = mm(reads_f[...], with_identity(ahead)) + mm(reads_b[...], with_identity(back))
     mixed = mixed[:, width:]
     centre = mixed - jnp.mean(mixed, axis=-1, keepdims=True)
     scaled = centre * lax.rsqrt(jnp.mean(centre * centre, axis=-1, keepdims=True) + 1e-05)
-    grouped = scaled * gain
-    split = grouped.reshape(chips, 2, -1, width)
-    results = []
-    for use in (core == 0, core != 0):
+    split = (scaled * gain[...]).reshape(own.shape[0], 2, -1, width)
+    for out, use in ((own, core[0] == 0), (away, core[0] != 0)):
         rows = jnp.where(use, split[:, 0], split[:, 1]).reshape(-1, width)
-        results.append(mm(rows.astype(BF16), w_output, None).astype(BF16))
-    return results
-
-
-def output_kernel(place, core, arrived, before, after, reads_f, reads_b, gain, w_output, own, away):
-    values = output_values(
-        place[0],
-        core[0],
-        [arrived[k] for k in range(arrived.shape[0])],
-        before[...],
-        after[...],
-        reads_f[...],
-        reads_b[...],
-        gain[...],
-        w_output[...],
-        own.shape[0],
-    )
-    for out, value in zip((own, away), values):
-        out[...] = value.reshape(out.shape)
-
-
-def down_block(hidden, down, parity, width, y):
-    columns = pl.ds(pl.multiple_of((2 * y + parity) * width, width), width)
-    return mm(hidden, down[:, columns], None).astype(BF16)
-
-
-def expert_kernel(width, core, arrived, swapped, gate, up, down, hidden, away):
+        out[...] = mm(rows.astype(BF16), w_output[...], None).astype(BF16).reshape(out.shape)
+
+
+def sort_kernel(width, core, gate, down, held, own, away):
+    held[...] = gate[...]
+    for out, parity in ((own, core[0]), (away, 1 - core[0])):
+        for y in range(out.shape[1] // width):
+            columns = pl.ds(pl.multiple_of((2 * y + parity) * width, width), width)
+            out[:, y * width : (y + 1) * width] = down[:, columns]
+
+
+def expert_kernel(core, arrived, swapped, gate, up, hidden):
     half = arrived.shape[1]
     at = core[0]
-    near = pl.ds(pl.multiple_of(at * half, half), half)
-    far = pl.ds(pl.multiple_of((1 - at) * half, half), half)
-    pairs = [(arrived[...], near), (swapped[...], far)]
+    near_rows = pl.ds(pl.multiple_of(at * half, half), half)
+    far_rows = pl.ds(pl.multiple_of((1 - at) * half, half), half)
+    pairs = [(arrived[...], near_rows), (swapped[...], far_rows)]
     gated = sum(mm(value, gate[where, :], None) for value, where in pairs)
     raised = sum(mm(value, up[where, :], None) for value, where in pairs)
-    inner = (gated / (1.0 + jnp.exp(-gated)) * raised).astype(BF16)
-    hidden[...] = inner
-    for y in range(half // width):
-        away[:, y * width : (y + 1) * width] = down_block(inner, down, 1 - at, width, y)
-
-
-def pair_kernel(width, core, hidden, landed, down, out):
-    inner = hidden[...]
-    for y in range(out.shape[1] // width):
-        columns = slice(y * width, (y + 1) * width)
-        part = down_block(inner, down, core[0], width, y).astype(F32)
-        out[:, columns] = (part + landed[:, columns].astype(F32)).astype(BF16)
+    hidden[...] = (gated / (1.0 + jnp.exp(-gated)) * raised).astype(BF16)
+
+
+def pair_kernel(hidden, landed, own, other, out):
+    rows = jnp.concatenate([hidden[...], landed[...]], axis=1)
+    for k in range(0, out.shape[1], BLOCK):
+        columns = slice(k, k + BLOCK)
+        weight = jnp.concatenate([own[:, columns], other[:, columns]], axis=0)
+        out[:, columns] = mm(rows, weight, None).astype(BF16)
 
 
 def combine_kernel(returned, weighing, own, landed, out):
@@ -270,10 +258,10 @@
     weighed = mm_tn(weighing[...], returned[...], None).astype(BF16)
     for y in range(chips):
         out[y, :tokens] = weighed[:, y * width : (y + 1) * width]
-        joined = own[y].astype(F32) + landed[y].astype(F32)
+        total = own[y].astype(F32) + landed[y].astype(F32)
         for k in range(own.shape[2] // width):
             rows = slice(tokens + k * each, tokens + (k + 1) * each)
-            out[y, rows] = joined[:, k * width : (k + 1) * width].astype(BF16)
+            out[y, rows] = total[:, k * width : (k + 1) * width].astype(BF16)
 
 
 def finish_kernel(shares, mixed, moe):
@@ -365,9 +353,11 @@
     place, lane = (lax.axis_index("ep"), lax.axis_index("tp"))
     core = lane & 1
     chips = tp // 2
-    across = ROW
-    rows = experts // across
-    high, low = (place // across, place % across)
+    across = 4
+    runs = experts // across
+    run = place // across
+    trade = lambda value, bit: lax.ppermute(value, "ep", [(k, k ^ bit) for k in range(experts)])
+    upper = lambda bit: scalar((place & bit) != 0)
     swap = [(k, k ^ 1) for k in range(tp)]
     tokens, model = moe_rows.shape
     slots = 4 * tokens // experts
@@ -409,23 +399,37 @@
         far(decay_shift.T),
     )
 
-    others = [
-        lax.ppermute(
-            both,
-            "ep",
-            [(k, k // across * across + (k + m) % across) for k in range(experts)],
-        )
-        for m in range(1, across)
-    ]
+    theirs = trade(both, 1)
+    total, before, after = call(
+        first_kernel,
+        (near(shape((2 * width, 2 * width), BF16)), wide, wide),
+        (upper(1),),
+        near(both),
+        near(theirs),
+    )
+    theirs = trade(total, 2)
     sent, before, after = call(
-        row_kernel,
-        (near(shape((rows, width, 2 * width), BF16)), wide, wide),
-        (scalar(low), scalar(high)),
-        near(both),
-        *[near(other) for other in others],
-    )
-
-    arrived, sent = lax.optimization_barrier((arrived, sent))
+        send_kernel,
+        (near(shape((runs, width, 2 * width), BF16)), wide, wide),
+        (upper(2), scalar(run)),
+        near(total),
+        near(theirs),
+        far(before),
+        far(after),
+    )
+
+    inner = exp_gate.shape[2]
+    columns = far(shape((inner, half), BF16))
+    gate, down_own, down_away = call(
+        functools.partial(sort_kernel, piece),
+        (near(shape((model, inner), BF16)), columns, columns),
+        (scalar(core),),
+        far(exp_gate[0]),
+        far(exp_down[0]),
+    )
+    down_other = lax.ppermute(down_away, "tp", swap)
+
+    arrived, sent, down_other = lax.optimization_barrier((arrived, sent, down_other))
 
     carried = lax.all_to_all(
         sent,
@@ -433,29 +437,28 @@
         split_axis=0,
         concat_axis=0,
         tiled=True,
-        axis_index_groups=[[z * across + x for z in range(rows)] for x in range(across)],
+        axis_index_groups=[[z * across + x for z in range(runs)] for x in range(across)],
     )
 
     swapped = lax.ppermute(arrived, "tp", swap)
-    inner = exp_gate.shape[2]
-    hidden, away = call(
-        functools.partial(expert_kernel, piece),
-        (near(shape((experts * slots, inner), BF16)), near(shape((experts * slots, half), BF16))),
+    hidden = call(
+        expert_kernel,
+        near(shape((experts * slots, inner), BF16)),
         (scalar(core),),
         near(arrived),
         near(swapped),
-        far(exp_gate[0]),
+        near(gate),
         near(exp_up[0]),
-        near(exp_down[0]),
-    )
-    landed = lax.ppermute(away, "tp", swap)
+    )
+    landed = lax.ppermute(hidden, "tp", swap)
     paired = call(
-        functools.partial(pair_kernel, piece),
+        pair_kernel,
         near(shape((experts * slots, half), BF16)),
-        (scalar(core),),
+        (),
         near(hidden),
         near(landed),
-        near(exp_down[0]),
+        near(down_own),
+        near(down_other),
     )
 
     returned = lax.all_to_all(
@@ -466,7 +469,7 @@
     own_rows, away_rows = call(
         output_kernel,
         (near(shares), near(shares)),
-        (scalar(high), scalar(core)),
+        (scalar(run), scalar(core)),
         near(carried),
         far(before),
         far(after),

time: 127 us -> 129 us (1.016)
  starting transfers between devices: 37.2 us -> 39.8 us
  waiting for transfers between devices: 40.5 us -> 38.5 us
    all_to_all x1, starting transfers between devices: 4.45 us -> 7.5 us  [shards(): lax.all_to_all(sent, 'ep', split_axis=0, concat_axis=0, tiled=True, axis_...]
    all_to_all x1, waiting for transfers between devices: 7.88 us -> 5.83 us  [shards(): lax.all_to_all(sent, 'ep', split_axis=0, concat_axis=0, tiled=True, axis_...]
    all_to_all x1, waiting for transfers between devices: 2.05 us -> 0.01 us  [shards(): lax.all_to_all(buffer.reshape(experts, slots, half), 'ep', split_axis=0,...]
    ppermute x4, waiting for transfers between devices: 5.21 us -> 7.17 us  [the longest x2 7.16 us: shards(): lax.ppermute(value, 'ep', [(k, k ^ bit) for k in range(experts)])]
    pallas_call x8 -> x10, Pallas kernels: 25.6 us -> 25.2 us  [call(): pl.pallas_call(kernel, out_shape=outs, in_specs=[smem] * len(scalars) + [...]
  transfers between devices with their start and end apart: 9 -> 9, of which waited for: 7 -> 6; matrix products, arithmetic and copies ran while one was open for 0% -> 0% of each run, Pallas kernels for 13% -> 15%
where the time goes in v3:
time: 129 us; the launch traced here: 128 us
  starting transfers between devices  39.8 us (31%)
  waiting for transfers between devices  38.5 us (30%)
  Pallas kernels  25.2 us (20%)
  blocking collectives  22.7 us (18%)
    pallas_call x10, Pallas kernels, call(): pl.pallas_call(kernel, out_shape=outs, in_specs=[smem] * len(scalars) + [...  25.2 us
    all_to_all x1, blocking collectives, shards(): lax.all_to_all(parts, 'tp', split_axis=0, concat_axis=0, tiled=True, axis...  22.7 us
    all_to_all x1, waiting for transfers between devices, shards(): lax.all_to_all(paired.reshape(experts, slots, half), 'ep', split_axis=0,...  21.4 us
    all_to_all x1, starting transfers between devices, shards(): lax.all_to_all(buffer.reshape(experts, slots, half), 'ep', split_axis=0,...  13.4 us
    all_to_all x1, starting transfers between devices, shards(): lax.all_to_all(sent, 'ep', split_axis=0, concat_axis=0, tiled=True, axis_...  7.5 us
    ppermute x2, waiting for transfers between devices, shards(): lax.ppermute(value, 'ep', [(k, k ^ bit) for k in range(experts)])  7.16 us
    ppermute x2, starting transfers between devices, shards(): lax.ppermute(value, 'ep', [(k, k ^ bit) for k in range(experts)])  6.31 us
    all_to_all x1, waiting for transfers between devices, shards(): lax.all_to_all(sent, 'ep', split_axis=0, concat_axis=0, tiled=True, axis_...  5.83 us
  transfers between devices with their start and end apart: 9, of which 6 were waited for; matrix products, arithmetic and copies ran while one was open for 0% of the time, Pallas kernels for 15%

profile of v3, /device:TPU:6, one launch (start us, length us, event | category | flops | bytes accessed | tf_op | source)
XLA Modules:
  0.0 128.1 jit_solution(17553701038038451399)
XLA Ops:
  0.6 2.7 %shard_map.203 = (bf16[512,1024]{1,0:T(8,128)(2,1)}, bf16[512,128]{1,0:T(8,128)(2,1)}) custom-call(s32[1]{0:T(128)} %bitcast.core, bf16[128,2048]{1,0:T(8,128)(2,1)} %rows.1, f32[1,2048]{1,0:T(1,128)} %bitcast.33, s32[2,128]{1,0:T(2,128)} %bitcast.35, f32[2,128]{1,0:T(2,128)} %bitcast.36), custom_call_target="tpu_custom_call" | custom-call | tf_op jit(solution)/shard_map/pallas_call | solution.py:321
  3.3 13.4 %all-to-all-start = ((bf16[32,16,1024]{2,1,0:T(8,128)(2,1)}), bf16[32,16,1024]{2,1,0:T(8,128)(2,1)S(1)}, u32[]{:S(2)}, u32[]{:S(2)}) async-start(bf16[32,16,1024]{2,1,0:T(8,128)(2,1)} %bitcast.4), calls=%async_computation | async-start | bytes 2097152 | tf_op jit(solution)/shard_map/all_to_all | solution.py:379
  16.8 2.8 %shard_map.207 = (bf16[2048,256]{1,0:T(8,128)(2,1)S(1)}, bf16[256,1024]{1,0:T(8,128)(2,1)}, bf16[256,1024]{1,0:T(8,128)(2,1)}) custom-call(s32[1]{0:T(128)} %bitcast.core, bf16[2048,256]{1,0:T(8,128)(2,1)} %bitcast.27, bf16[256,2048]{1,0:T(8,128)(2,1)} %bitcast.28), custom_call_target="tpu_custom_call" | custom-call | tf_op jit(solution)/shard_map/pallas_call | solution.py:321
  19.5 2.0 %collective-permute-start.2 = (bf16[256,1024]{1,0:T(8,128)(2,1)}, bf16[256,1024]{1,0:T(8,128)(2,1)}, u32[]{:S(2)}, u32[]{:S(2)}) collective-permute-start(bf16[256,1024]{1,0:T(8,128)(2,1)} %get-tuple-element.27), channel_id=1, source_target_pairs={{0,1},{1,0},{2,3},{3,2},{4,5},{5,4},{6,7},{7,6},{8,9},{9,8},{10,11... | collective-permute-start | bytes 1572872 | tf_op jit(solution)/shard_map/ppermute | solution.py:430
  21.6 8.5 %shard_map.204 = (f32[128,128]{1,0:T(8,128)}, f32[128,128]{1,0:T(8,128)}, bf16[128,128]{1,0:T(8,128)(2,1)S(1)}) custom-call(bf16[128,2048]{1,0:T(8,128)(2,1)} %refs_0_.1, f32[1,2048]{1,0:T(1,128)} %bitcast.34, bf16[64,2048]{1,0:T(8,128)(2,1)} %bitcast.29, bf16[64,2048]{1,0:T(8,128)(2,1)} %bitcast.30, bf16[64,2048]{1,0:T(8,128)(2,1)} %bitcast.31, ...), custom_call_target="tpu_custom_call" | custom-call | tf_op jit(solution)/shard_map/pallas_call | solution.py:321
  30.1 2.8 %collective-permute-start = (bf16[128,128]{1,0:T(8,128)(2,1)S(1)}, bf16[128,128]{1,0:T(8,128)(2,1)S(1)}, u32[]{:S(2)}, u32[]{:S(2)}) collective-permute-start(bf16[128,128]{1,0:T(8,128)(2,1)S(1)} %get-tuple-element.22.mine), channel_id=1, source_target_pairs={{0,16},{16,0},{32,48},{48,32},{64,80},{80,64},{96,112},{112,96},{1... | collective-permute-start | bytes 98312 | tf_op jit(solution)/shard_map/ppermute | solution.py:359
  32.9 3.4 %collective-permute-done.theirs = bf16[128,128]{1,0:T(8,128)(2,1)S(1)} collective-permute-done((bf16[128,128]{1,0:T(8,128)(2,1)S(1)}, bf16[128,128]{1,0:T(8,128)(2,1)S(1)}, u32[]{:S(2)}, u32[]{:S(2)}) %collective-permute-start) | collective-permute-done | bytes 32800 | tf_op jit(solution)/shard_map/ppermute | solution.py:359
  36.3 0.8 shard_map.205
  37.1 3.6 %collective-permute-start.1 = (bf16[128,128]{1,0:T(8,128)(2,1)S(1)}, bf16[128,128]{1,0:T(8,128)(2,1)S(1)}, u32[]{:S(2)}, u32[]{:S(2)}) collective-permute-start(bf16[128,128]{1,0:T(8,128)(2,1)S(1)} %get-tuple-element.23.mine), channel_id=1, source_target_pairs={{0,32},{16,48},{32,0},{48,16},{64,96},{80,112},{96,64},{112,80},{1... | collective-permute-start | bytes 98312 | tf_op jit(solution)/shard_map/ppermute | solution.py:359
  40.7 3.7 %collective-permute-done.1.theirs = bf16[128,128]{1,0:T(8,128)(2,1)S(1)} collective-permute-done((bf16[128,128]{1,0:T(8,128)(2,1)S(1)}, bf16[128,128]{1,0:T(8,128)(2,1)S(1)}, u32[]{:S(2)}, u32[]{:S(2)}) %collective-permute-start.1) | collective-permute-done | bytes 32800 | tf_op jit(solution)/shard_map/ppermute | solution.py:359
  44.4 1.6 %shard_map.206 = (bf16[8,64,128]{2,1,0:T(8,128)(2,1)}, f32[64,128]{1,0:T(8,128)}, f32[64,128]{1,0:T(8,128)}) custom-call(s32[1]{0:T(128)} %bitcast.6.high, s32[1]{0:T(128)} %bitcast.7.run, bf16[128,128]{1,0:T(8,128)(2,1)S(1)} %get-tuple-element.23.mine, bf16[128,128]{1,0:T(8,128)(2,1)S(1)} %collective-permute-done.1.theirs, ...), custom_call_target="tpu_custom_call" | custom-call | tf_op jit(solution)/shard_map/pallas_call | solution.py:321
  46.0 0.0 collective-permute-done.2.other
  46.0 0.0 all-to-all-done
  46.0 1.9 %collective-permute-start.3 = (bf16[512,1024]{1,0:T(8,128)(2,1)S(1)}, bf16[512,1024]{1,0:T(8,128)(2,1)S(1)}, u32[]{:S(2)}, u32[]{:S(2)}) collective-permute-start(bf16[512,1024]{1,0:T(8,128)(2,1)S(1)} %bitcast.23), channel_id=1, source_target_pairs={{0,1},{1,0},{2,3},{3,2},{4,5},{5,4},{6,7},{7,6},{8,9},{9,8},{10,11... | collective-permute-start | bytes 3145736 | tf_op jit(solution)/shard_map/ppermute | solution.py:443
  47.9 2.6 %collective-permute-done.3.swapped = bf16[512,1024]{1,0:T(8,128)(2,1)S(1)} collective-permute-done((bf16[512,1024]{1,0:T(8,128)(2,1)S(1)}, bf16[512,1024]{1,0:T(8,128)(2,1)S(1)}, u32[]{:S(2)}, u32[]{:S(2)}) %collective-permute-start.3) | collective-permute-done | bytes 1048608 | tf_op jit(solution)/shard_map/ppermute | solution.py:443
  50.5 0.0 copy-done
  50.5 1.3 shard_map.208.hidden
  51.8 2.0 %collective-permute-start.4 = (bf16[512,256]{1,0:T(8,128)(2,1)S(1)}, bf16[512,256]{1,0:T(8,128)(2,1)S(1)}, u32[]{:S(2)}, u32[]{:S(2)}) collective-permute-start(bf16[512,256]{1,0:T(8,128)(2,1)S(1)} %shard_map.208.hidden), channel_id=1, source_target_pairs={{0,1},{1,0},{2,3},{3,2},{4,5},{5,4},{6,7},{7,6},{8,9},{9,8},{10,11... | collective-permute-start | bytes 786440 | tf_op jit(solution)/shard_map/ppermute | solution.py:453
  53.9 7.5 %all-to-all-start.2 = ((bf16[8,64,128]{2,1,0:T(8,128)(2,1)}), bf16[8,64,128]{2,1,0:T(8,128)(2,1)S(1)}, u32[]{:S(2)}, u32[]{:S(2)}) async-start(bf16[8,64,128]{2,1,0:T(8,128)(2,1)} %get-tuple-element.33), calls=%async_computation.2 | async-start | bytes 262144 | tf_op jit(solution)/shard_map/all_to_all | solution.py:434
  61.4 0.0 collective-permute-done.4.landed
  61.4 0.0 copy-start.1
  61.4 1.0 copy-done.1
  62.4 2.7 %shard_map.209 = bf16[512,1024]{1,0:T(8,128)(2,1)} custom-call(bf16[512,256]{1,0:T(8,128)(2,1)S(1)} %shard_map.208.hidden, bf16[512,256]{1,0:T(8,128)(2,1)S(1)} %collective-permute-done.4.landed, bf16[256,1024]{1,0:T(8,128)(2,1)S(1)} %copy-done.1, bf16[256,1024]{1,0:T(8,128)(2,1)} %collective-permute-done.2.other), custom_call_target="tpu_custom_call" | custom-call | tf_op jit(solution)/shard_map/pallas_call | solution.py:321
  65.2 5.8 %all-to-all-done.2.arrived = bf16[8,64,128]{2,1,0:T(8,128)(2,1)S(1)} async-done(((bf16[8,64,128]{2,1,0:T(8,128)(2,1)}), bf16[8,64,128]{2,1,0:T(8,128)(2,1)S(1)}, u32[]{:S(2)}, u32[]{:S(2)}) %all-to-all-start.2) | async-done | bytes 131104 | tf_op jit(solution)/shard_map/all_to_all | solution.py:434
  71.0 4.7 %all-to-all-start.1 = ((bf16[32,16,1024]{2,1,0:T(8,128)(2,1)}), bf16[32,16,1024]{2,1,0:T(8,128)(2,1)S(1)}, u32[]{:S(2)}, u32[]{:S(2)}) async-start(bf16[32,16,1024]{2,1,0:T(8,128)(2,1)} %bitcast.20), calls=%async_computation.1 | async-start | bytes 2097152 | tf_op jit(solution)/shard_map/all_to_all | solution.py:464
  75.7 2.9 %shard_map.210 = (bf16[8,8,2048]{2,1,0:T(8,128)(2,1)S(1)}, bf16[8,8,2048]{2,1,0:T(8,128)(2,1)S(1)}) custom-call(s32[1]{0:T(128)} %bitcast.7.run, s32[1]{0:T(128)} %bitcast.core, bf16[8,64,128]{2,1,0:T(8,128)(2,1)S(1)} %all-to-all-done.2.arrived, f32[64,128]{1,0:T(8,128)} %get-tuple-element.34.before, f32[64,128]{1,0:T(8,128)} %get-tuple-element.35.after, ...), custom_call_target="tpu_custom_call" | custom-call | tf_op jit(solution)/shard_map/pallas_call | solution.py:321
  78.5 1.9 %collective-permute-start.5 = (bf16[8,8,2048]{2,1,0:T(8,128)(2,1)S(1)}, bf16[8,8,2048]{2,1,0:T(8,128)(2,1)S(1)}, u32[]{:S(2)}, u32[]{:S(2)}) collective-permute-start(bf16[8,8,2048]{2,1,0:T(8,128)(2,1)S(1)} %get-tuple-element.39), channel_id=1, source_target_pairs={{0,1},{1,0},{2,3},{3,2},{4,5},{5,4},{6,7},{7,6},{8,9},{9,8},{10,11... | collective-permute-start | bytes 786440 | tf_op jit(solution)/shard_map/ppermute | solution.py:481
  80.5 1.5 %collective-permute-done.5.landed = bf16[8,8,2048]{2,1,0:T(8,128)(2,1)S(1)} collective-permute-done((bf16[8,8,2048]{2,1,0:T(8,128)(2,1)S(1)}, bf16[8,8,2048]{2,1,0:T(8,128)(2,1)S(1)}, u32[]{:S(2)}, u32[]{:S(2)}) %collective-permute-start.5) | collective-permute-done | bytes 262176 | tf_op jit(solution)/shard_map/ppermute | solution.py:481
  82.0 21.4 %all-to-all-done.1 = bf16[32,16,1024]{2,1,0:T(8,128)(2,1)S(1)} async-done(((bf16[32,16,1024]{2,1,0:T(8,128)(2,1)}), bf16[32,16,1024]{2,1,0:T(8,128)(2,1)S(1)}, u32[]{:S(2)}, u32[]{:S(2)}) %all-to-all-start.1) | async-done | bytes 1048608 | tf_op jit(solution)/shard_map/all_to_all | solution.py:464
  103.4 1.3 shard_map.211
  104.7 22.7 %all_to_all.20.shares = bf16[8,256,128]{2,1,0:T(8,128)(2,1)S(1)} all-to-all(bf16[8,256,128]{2,1,0:T(8,128)(2,1)S(1)} %shard_map.211), channel_id=1, replica_groups={{0,2,4,6,8,10,12,14},{1,3,5,7,9,11,13,15},{16,18,20,22,24,26,28,30},{17..., dimensions={0} | all-to-all | bytes 1048576 | tf_op jit(solution)/shard_map/all_to_all | solution.py:492
  127.4 0.7 shard_map.212
  (1 shorter events, 0.0 us)
Async XLA Ops:
  3.3 42.7 %all-to-all-start = ((bf16[32,16,1024]{2,1,0:T(8,128)(2,1)}), bf16[32,16,1024]{2,1,0:T(8,128)(2,1)S(1)}, u32[]{:S(2)}, u32[]{:S(2)}) async-start(bf16[32,16,1024]{2,1,0:T(8,128)(2,1)} %bitcast.4), calls=%async_computation | async-start | bytes 2097152 | tf_op jit(solution)/shard_map/all_to_all | solution.py:379
  19.5 31.0 %copy-start = (bf16[1,2048,256]{2,1,0:T(8,128)(2,1)S(1)}, bf16[1,2048,256]{2,1,0:T(8,128)(2,1)}, u32[]{:S(2)}) copy-start(bf16[1,2048,256]{2,1,0:T(8,128)(2,1)} %param.38) | copy-start | bytes 3145732
  19.5 26.5 %collective-permute-start.2 = (bf16[256,1024]{1,0:T(8,128)(2,1)}, bf16[256,1024]{1,0:T(8,128)(2,1)}, u32[]{:S(2)}, u32[]{:S(2)}) collective-permute-start(bf16[256,1024]{1,0:T(8,128)(2,1)} %get-tuple-element.27), channel_id=1, source_target_pairs={{0,1},{1,0},{2,3},{3,2},{4,5},{5,4},{6,7},{7,6},{8,9},{9,8},{10,11... | collective-permute-start | bytes 1572872 | tf_op jit(solution)/shard_map/ppermute | solution.py:430
  30.1 6.2 %collective-permute-start = (bf16[128,128]{1,0:T(8,128)(2,1)S(1)}, bf16[128,128]{1,0:T(8,128)(2,1)S(1)}, u32[]{:S(2)}, u32[]{:S(2)}) collective-permute-start(bf16[128,128]{1,0:T(8,128)(2,1)S(1)} %get-tuple-element.22.mine), channel_id=1, source_target_pairs={{0,16},{16,0},{32,48},{48,32},{64,80},{80,64},{96,112},{112,96},{1... | collective-permute-start | bytes 98312 | tf_op jit(solution)/shard_map/ppermute | solution.py:359
  37.1 7.3 %collective-permute-start.1 = (bf16[128,128]{1,0:T(8,128)(2,1)S(1)}, bf16[128,128]{1,0:T(8,128)(2,1)S(1)}, u32[]{:S(2)}, u32[]{:S(2)}) collective-permute-start(bf16[128,128]{1,0:T(8,128)(2,1)S(1)} %get-tuple-element.23.mine), channel_id=1, source_target_pairs={{0,32},{16,48},{32,0},{48,16},{64,96},{80,112},{96,64},{112,80},{1... | collective-permute-start | bytes 98312 | tf_op jit(solution)/shard_map/ppermute | solution.py:359
  46.0 4.6 %collective-permute-start.3 = (bf16[512,1024]{1,0:T(8,128)(2,1)S(1)}, bf16[512,1024]{1,0:T(8,128)(2,1)S(1)}, u32[]{:S(2)}, u32[]{:S(2)}) collective-permute-start(bf16[512,1024]{1,0:T(8,128)(2,1)S(1)} %bitcast.23), channel_id=1, source_target_pairs={{0,1},{1,0},{2,3},{3,2},{4,5},{5,4},{6,7},{7,6},{8,9},{9,8},{10,11... | collective-permute-start | bytes 3145736 | tf_op jit(solution)/shard_map/ppermute | solution.py:443
  51.8 9.6 %collective-permute-start.4 = (bf16[512,256]{1,0:T(8,128)(2,1)S(1)}, bf16[512,256]{1,0:T(8,128)(2,1)S(1)}, u32[]{:S(2)}, u32[]{:S(2)}) collective-permute-start(bf16[512,256]{1,0:T(8,128)(2,1)S(1)} %shard_map.208.hidden), channel_id=1, source_target_pairs={{0,1},{1,0},{2,3},{3,2},{4,5},{5,4},{6,7},{7,6},{8,9},{9,8},{10,11... | collective-permute-start | bytes 786440 | tf_op jit(solution)/shard_map/ppermute | solution.py:453
  53.9 17.1 %all-to-all-start.2 = ((bf16[8,64,128]{2,1,0:T(8,128)(2,1)}), bf16[8,64,128]{2,1,0:T(8,128)(2,1)S(1)}, u32[]{:S(2)}, u32[]{:S(2)}) async-start(bf16[8,64,128]{2,1,0:T(8,128)(2,1)} %get-tuple-element.33), calls=%async_computation.2 | async-start | bytes 262144 | tf_op jit(solution)/shard_map/all_to_all | solution.py:434
  61.4 1.0 copy-start.1
  71.0 32.4 %all-to-all-start.1 = ((bf16[32,16,1024]{2,1,0:T(8,128)(2,1)}), bf16[32,16,1024]{2,1,0:T(8,128)(2,1)S(1)}, u32[]{:S(2)}, u32[]{:S(2)}) async-start(bf16[32,16,1024]{2,1,0:T(8,128)(2,1)} %bitcast.20), calls=%async_computation.1 | async-start | bytes 2097152 | tf_op jit(solution)/shard_map/all_to_all | solution.py:464
  78.5 3.4 %collective-permute-start.5 = (bf16[8,8,2048]{2,1,0:T(8,128)(2,1)S(1)}, bf16[8,8,2048]{2,1,0:T(8,128)(2,1)S(1)}, u32[]{:S(2)}, u32[]{:S(2)}) collective-permute-start(bf16[8,8,2048]{2,1,0:T(8,128)(2,1)S(1)} %get-tuple-element.39), channel_id=1, source_target_pairs={{0,1},{1,0},{2,3},{3,2},{4,5},{5,4},{6,7},{7,6},{8,9},{9,8},{10,11... | collective-permute-start | bytes 786440 | tf_op jit(solution)/shard_map/ppermute | solution.py:481

commit v4 on v3

--- a/solution.py
+++ b/solution.py
@@ -252,28 +252,26 @@
         out[:, columns] = mm(rows, weight, None).astype(BF16)
 
 
-def combine_kernel(returned, weighing, own, landed, out):
-    chips, each, width = own.shape[0], own.shape[1], out.shape[2]
-    tokens = weighing.shape[1]
+def halve_kernel(bit, mine, landed, keep, send):
+    for k in range(keep.shape[0]):
+        total = [(mine[2 * k + m].astype(F32) + landed[2 * k + m].astype(F32)) for m in range(2)]
+        keep[k] = jnp.where(bit[0] != 0, total[1], total[0]).astype(BF16)
+        send[k] = jnp.where(bit[0] != 0, total[0], total[1]).astype(BF16)
+
+
+def combine_kernel(returned, weighing, out):
+    width = out.shape[2]
     weighed = mm_tn(weighing[...], returned[...], None).astype(BF16)
-    for y in range(chips):
-        out[y, :tokens] = weighed[:, y * width : (y + 1) * width]
-        total = own[y].astype(F32) + landed[y].astype(F32)
-        for k in range(own.shape[2] // width):
-            rows = slice(tokens + k * each, tokens + (k + 1) * each)
-            out[y, rows] = total[:, k * width : (k + 1) * width].astype(BF16)
-
-
-def finish_kernel(shares, mixed, moe):
-    chips, width = shares.shape[0], shares.shape[2]
-    tokens, each = moe.shape[0], mixed.shape[0]
+    for y in range(out.shape[0]):
+        out[y] = weighed[:, y * width : (y + 1) * width]
+
+
+def finish_kernel(shares, keep, landed, mixed, moe):
     total = shares[0].astype(F32)
-    for y in range(1, chips):
+    for y in range(1, shares.shape[0]):
         total = total + shares[y].astype(F32)
-    moe[...] = total[:tokens].astype(BF16)
-    for k in range(mixed.shape[1] // width):
-        rows = slice(tokens + k * each, tokens + (k + 1) * each)
-        mixed[:, k * width : (k + 1) * width] = total[rows].astype(BF16)
+    moe[...] = total.astype(BF16)
+    mixed[...] = (keep[0].astype(F32) + landed[0].astype(F32)).astype(BF16)
 
 
 def route_values(routes, weights, experts, slots):
@@ -351,7 +349,7 @@
 ):
     experts, tp = (lax.axis_size("ep"), lax.axis_size("tp"))
     place, lane = (lax.axis_index("ep"), lax.axis_index("tp"))
-    core = lane & 1
+    core, chip = (lane & 1, lane >> 1)
     chips = tp // 2
     across = 4
     runs = experts // across
@@ -478,16 +476,26 @@
         far(out_gain.reshape(1, -1)),
         far(w_output),
     )
-    landed_rows = lax.ppermute(away_rows, "tp", swap)
+    keep, landed = (own_rows, lax.ppermute(away_rows, "tp", swap))
+    bit = 1
+    while bit < chips:
+        part = near(shape((keep.shape[0] // 2, tokens // tp, model), BF16))
+        keep, send = call(
+            halve_kernel,
+            (part, part),
+            (scalar((chip & bit) != 0),),
+            near(keep),
+            near(landed),
+        )
+        landed = lax.ppermute(send, "tp", [(k, k ^ (2 * bit)) for k in range(tp)])
+        bit *= 2
 
     parts = call(
         combine_kernel,
-        near(shape((chips, 2 * tokens, piece), BF16)),
+        near(shape((chips, tokens, piece), BF16)),
         (),
         near(returned),
         far(weighing),
-        near(own_rows),
-        near(landed_rows),
     )
     parts = lax.all_to_all(
         parts,
@@ -502,6 +510,8 @@
         (shape((tokens // tp, model), BF16), shape((tokens, piece), BF16)),
         (),
         near(parts),
+        near(keep),
+        near(landed),
     )
     return (mix_out, moe_out)
 

time: 129 us -> 141 us (1.093)
  blocking collectives: 22.7 us -> 0 us
  starting transfers between devices: 39.8 us -> 62.1 us
  waiting for transfers between devices: 38.5 us -> 49.7 us
    all_to_all x1 -> x0, blocking collectives: 22.7 us -> none  [shards(): lax.all_to_all(parts, 'tp', split_axis=0, concat_axis=0, tiled=True, axis...]
    ppermute x1 -> x4, starting transfers between devices: 1.92 us -> 17.1 us  [the longest x3 15.2 us: shards(): landed = lax.ppermute(send, 'tp', [(k, k ^ 2 * bit) for k in range(tp)])]
    ppermute x1 -> x4, waiting for transfers between devices: 1.5 us -> 11.2 us  [the longest x3 11.2 us: shards(): landed = lax.ppermute(send, 'tp', [(k, k ^ 2 * bit) for k in range(tp)])]
    all_to_all x0 -> x1, starting transfers between devices: none -> 7.13 us  [shards(): lax.all_to_all(parts, 'tp', split_axis=0, concat_axis=0, tiled=True, axis...]
    all_to_all x1, waiting for transfers between devices: 21.4 us -> 22.9 us  [shards(): lax.all_to_all(paired.reshape(experts, slots, half), 'ep', split_axis=0,...]
    pallas_call x10 -> x13, Pallas kernels: 25.2 us -> 26.1 us  [call(): pl.pallas_call(kernel, out_shape=outs, in_specs=[smem] * len(scalars) + [...]
  transfers between devices with their start and end apart: 9 -> 13, of which waited for: 6 -> 8; matrix products, arithmetic and copies ran while one was open for 0% -> 0% of each run, Pallas kernels for 15% -> 15%
where the time goes in v4:
time: 141 us; the launch traced here: 140 us
  starting transfers between devices  62.1 us (44%)
  waiting for transfers between devices  49.7 us (35%)
  Pallas kernels  26.1 us (19%)
    pallas_call x13, Pallas kernels, call(): pl.pallas_call(kernel, out_shape=outs, in_specs=[smem] * len(scalars) + [...  26.1 us
    all_to_all x1, waiting for transfers between devices, shards(): lax.all_to_all(paired.reshape(experts, slots, half), 'ep', split_axis=0,...  22.9 us
    ppermute x3, starting transfers between devices, shards(): landed = lax.ppermute(send, 'tp', [(k, k ^ 2 * bit) for k in range(tp)])  15.2 us
    all_to_all x1, starting transfers between devices, shards(): lax.all_to_all(buffer.reshape(experts, slots, half), 'ep', split_axis=0,...  13.4 us
    ppermute x3, waiting for transfers between devices, shards(): landed = lax.ppermute(send, 'tp', [(k, k ^ 2 * bit) for k in range(tp)])  11.2 us
    all_to_all x1, starting transfers between devices, shards(): lax.all_to_all(sent, 'ep', split_axis=0, concat_axis=0, tiled=True, axis_...  7.48 us
    ppermute x2, waiting for transfers between devices, shards(): lax.ppermute(value, 'ep', [(k, k ^ bit) for k in range(experts)])  7.17 us
    all_to_all x1, starting transfers between devices, shards(): lax.all_to_all(parts, 'tp', split_axis=0, concat_axis=0, tiled=True, axis...  7.13 us
  transfers between devices with their start and end apart: 13, of which 8 were waited for; matrix products, arithmetic and copies ran while one was open for 0% of the time, Pallas kernels for 15%

profile of v4, /device:TPU:6, one launch (start us, length us, event | category | flops | bytes accessed | tf_op | source)
XLA Modules:
  0.0 139.6 jit_solution(13744237639553266413)
XLA Ops:
  0.6 2.7 %shard_map.203 = (bf16[512,1024]{1,0:T(8,128)(2,1)}, bf16[512,128]{1,0:T(8,128)(2,1)}) custom-call(s32[1]{0:T(128)} %bitcast.core, bf16[128,2048]{1,0:T(8,128)(2,1)} %rows.1, f32[1,2048]{1,0:T(1,128)} %bitcast.36, s32[2,128]{1,0:T(2,128)} %bitcast.38, f32[2,128]{1,0:T(2,128)} %bitcast.39), custom_call_target="tpu_custom_call" | custom-call | tf_op jit(solution)/shard_map/pallas_call | solution.py:319
  3.4 13.4 %all-to-all-start = ((bf16[32,16,1024]{2,1,0:T(8,128)(2,1)}), bf16[32,16,1024]{2,1,0:T(8,128)(2,1)S(1)}, u32[]{:S(2)}, u32[]{:S(2)}) async-start(bf16[32,16,1024]{2,1,0:T(8,128)(2,1)} %bitcast.4), calls=%async_computation | async-start | bytes 2097152 | tf_op jit(solution)/shard_map/all_to_all | solution.py:377
  16.8 2.8 %shard_map.207 = (bf16[2048,256]{1,0:T(8,128)(2,1)S(1)}, bf16[256,1024]{1,0:T(8,128)(2,1)}, bf16[256,1024]{1,0:T(8,128)(2,1)}) custom-call(s32[1]{0:T(128)} %bitcast.core, bf16[2048,256]{1,0:T(8,128)(2,1)} %bitcast.30, bf16[256,2048]{1,0:T(8,128)(2,1)} %bitcast.31), custom_call_target="tpu_custom_call" | custom-call | tf_op jit(solution)/shard_map/pallas_call | solution.py:319
  19.6 2.0 %collective-permute-start.2 = (bf16[256,1024]{1,0:T(8,128)(2,1)}, bf16[256,1024]{1,0:T(8,128)(2,1)}, u32[]{:S(2)}, u32[]{:S(2)}) collective-permute-start(bf16[256,1024]{1,0:T(8,128)(2,1)} %get-tuple-element.33), channel_id=1, source_target_pairs={{0,1},{1,0},{2,3},{3,2},{4,5},{5,4},{6,7},{7,6},{8,9},{9,8},{10,11... | collective-permute-start | bytes 1572872 | tf_op jit(solution)/shard_map/ppermute | solution.py:428
  21.6 8.5 %shard_map.204 = (f32[128,128]{1,0:T(8,128)}, f32[128,128]{1,0:T(8,128)}, bf16[128,128]{1,0:T(8,128)(2,1)S(1)}) custom-call(bf16[128,2048]{1,0:T(8,128)(2,1)} %refs_0_.1, f32[1,2048]{1,0:T(1,128)} %bitcast.37, bf16[64,2048]{1,0:T(8,128)(2,1)} %bitcast.32, bf16[64,2048]{1,0:T(8,128)(2,1)} %bitcast.33, bf16[64,2048]{1,0:T(8,128)(2,1)} %bitcast.34, ...), custom_call_target="tpu_custom_call" | custom-call | tf_op jit(solution)/shard_map/pallas_call | solution.py:319
  30.1 2.8 %collective-permute-start = (bf16[128,128]{1,0:T(8,128)(2,1)S(1)}, bf16[128,128]{1,0:T(8,128)(2,1)S(1)}, u32[]{:S(2)}, u32[]{:S(2)}) collective-permute-start(bf16[128,128]{1,0:T(8,128)(2,1)S(1)} %get-tuple-element.28.mine), channel_id=1, source_target_pairs={{0,16},{16,0},{32,48},{48,32},{64,80},{80,64},{96,112},{112,96},{1... | collective-permute-start | bytes 98312 | tf_op jit(solution)/shard_map/ppermute | solution.py:357
  32.9 3.4 %collective-permute-done.theirs = bf16[128,128]{1,0:T(8,128)(2,1)S(1)} collective-permute-done((bf16[128,128]{1,0:T(8,128)(2,1)S(1)}, bf16[128,128]{1,0:T(8,128)(2,1)S(1)}, u32[]{:S(2)}, u32[]{:S(2)}) %collective-permute-start) | collective-permute-done | bytes 32800 | tf_op jit(solution)/shard_map/ppermute | solution.py:357
  36.3 0.8 shard_map.205
  37.1 3.5 %collective-permute-start.1 = (bf16[128,128]{1,0:T(8,128)(2,1)S(1)}, bf16[128,128]{1,0:T(8,128)(2,1)S(1)}, u32[]{:S(2)}, u32[]{:S(2)}) collective-permute-start(bf16[128,128]{1,0:T(8,128)(2,1)S(1)} %get-tuple-element.29.mine), channel_id=1, source_target_pairs={{0,32},{16,48},{32,0},{48,16},{64,96},{80,112},{96,64},{112,80},{1... | collective-permute-start | bytes 98312 | tf_op jit(solution)/shard_map/ppermute | solution.py:357
  40.7 3.7 %collective-permute-done.1.theirs = bf16[128,128]{1,0:T(8,128)(2,1)S(1)} collective-permute-done((bf16[128,128]{1,0:T(8,128)(2,1)S(1)}, bf16[128,128]{1,0:T(8,128)(2,1)S(1)}, u32[]{:S(2)}, u32[]{:S(2)}) %collective-permute-start.1) | collective-permute-done | bytes 32800 | tf_op jit(solution)/shard_map/ppermute | solution.py:357
  44.4 1.6 %shard_map.206 = (bf16[8,64,128]{2,1,0:T(8,128)(2,1)}, f32[64,128]{1,0:T(8,128)}, f32[64,128]{1,0:T(8,128)}) custom-call(s32[1]{0:T(128)} %bitcast.6.high, s32[1]{0:T(128)} %bitcast.7.run, bf16[128,128]{1,0:T(8,128)(2,1)S(1)} %get-tuple-element.29.mine, bf16[128,128]{1,0:T(8,128)(2,1)S(1)} %collective-permute-done.1.theirs, ...), custom_call_target="tpu_custom_call" | custom-call | tf_op jit(solution)/shard_map/pallas_call | solution.py:319
  46.0 1.9 %collective-permute-start.3 = (bf16[512,1024]{1,0:T(8,128)(2,1)S(1)}, bf16[512,1024]{1,0:T(8,128)(2,1)S(1)}, u32[]{:S(2)}, u32[]{:S(2)}) collective-permute-start(bf16[512,1024]{1,0:T(8,128)(2,1)S(1)} %bitcast.26), channel_id=1, source_target_pairs={{0,1},{1,0},{2,3},{3,2},{4,5},{5,4},{6,7},{7,6},{8,9},{9,8},{10,11... | collective-permute-start | bytes 3145736 | tf_op jit(solution)/shard_map/ppermute | solution.py:441
  47.9 2.6 %collective-permute-done.3.swapped = bf16[512,1024]{1,0:T(8,128)(2,1)S(1)} collective-permute-done((bf16[512,1024]{1,0:T(8,128)(2,1)S(1)}, bf16[512,1024]{1,0:T(8,128)(2,1)S(1)}, u32[]{:S(2)}, u32[]{:S(2)}) %collective-permute-start.3) | collective-permute-done | bytes 1048608 | tf_op jit(solution)/shard_map/ppermute | solution.py:441
  50.6 1.3 shard_map.208.hidden
  51.9 2.0 %collective-permute-start.4 = (bf16[512,256]{1,0:T(8,128)(2,1)S(1)}, bf16[512,256]{1,0:T(8,128)(2,1)S(1)}, u32[]{:S(2)}, u32[]{:S(2)}) collective-permute-start(bf16[512,256]{1,0:T(8,128)(2,1)S(1)} %shard_map.208.hidden), channel_id=1, source_target_pairs={{0,1},{1,0},{2,3},{3,2},{4,5},{5,4},{6,7},{7,6},{8,9},{9,8},{10,11... | collective-permute-start | bytes 786440 | tf_op jit(solution)/shard_map/ppermute | solution.py:451
  53.9 7.5 %all-to-all-start.3 = ((bf16[8,64,128]{2,1,0:T(8,128)(2,1)}), bf16[8,64,128]{2,1,0:T(8,128)(2,1)S(1)}, u32[]{:S(2)}, u32[]{:S(2)}) async-start(bf16[8,64,128]{2,1,0:T(8,128)(2,1)} %get-tuple-element.39), calls=%async_computation.3 | async-start | bytes 262144 | tf_op jit(solution)/shard_map/all_to_all | solution.py:432
  61.4 1.0 copy-done.1
  62.4 2.8 %shard_map.209 = bf16[512,1024]{1,0:T(8,128)(2,1)} custom-call(bf16[512,256]{1,0:T(8,128)(2,1)S(1)} %shard_map.208.hidden, bf16[512,256]{1,0:T(8,128)(2,1)S(1)} %collective-permute-done.4.landed, bf16[256,1024]{1,0:T(8,128)(2,1)S(1)} %copy-done.1, bf16[256,1024]{1,0:T(8,128)(2,1)} %collective-permute-done.2.other), custom_call_target="tpu_custom_call" | custom-call | tf_op jit(solution)/shard_map/pallas_call | solution.py:319
  65.2 5.8 %all-to-all-done.3.arrived = bf16[8,64,128]{2,1,0:T(8,128)(2,1)S(1)} async-done(((bf16[8,64,128]{2,1,0:T(8,128)(2,1)}), bf16[8,64,128]{2,1,0:T(8,128)(2,1)S(1)}, u32[]{:S(2)}, u32[]{:S(2)}) %all-to-all-start.3) | async-done | bytes 131104 | tf_op jit(solution)/shard_map/all_to_all | solution.py:432
  71.0 4.7 %all-to-all-start.1 = ((bf16[32,16,1024]{2,1,0:T(8,128)(2,1)}), bf16[32,16,1024]{2,1,0:T(8,128)(2,1)S(1)}, u32[]{:S(2)}, u32[]{:S(2)}) async-start(bf16[32,16,1024]{2,1,0:T(8,128)(2,1)} %bitcast.20), calls=%async_computation.1 | async-start | bytes 2097152 | tf_op jit(solution)/shard_map/all_to_all | solution.py:462
  75.7 2.9 %shard_map.211 = (bf16[8,8,2048]{2,1,0:T(8,128)(2,1)S(1)}, bf16[8,8,2048]{2,1,0:T(8,128)(2,1)S(1)}) custom-call(s32[1]{0:T(128)} %bitcast.7.run, s32[1]{0:T(128)} %bitcast.core, bf16[8,64,128]{2,1,0:T(8,128)(2,1)S(1)} %all-to-all-done.3.arrived, f32[64,128]{1,0:T(8,128)} %get-tuple-element.40.before, f32[64,128]{1,0:T(8,128)} %get-tuple-element.41.after, ...), custom_call_target="tpu_custom_call" | custom-call | tf_op jit(solution)/shard_map/pallas_call | solution.py:319
  78.5 1.9 %collective-permute-start.5 = (bf16[8,8,2048]{2,1,0:T(8,128)(2,1)S(1)}, bf16[8,8,2048]{2,1,0:T(8,128)(2,1)S(1)}, u32[]{:S(2)}, u32[]{:S(2)}) collective-permute-start(bf16[8,8,2048]{2,1,0:T(8,128)(2,1)S(1)} %get-tuple-element.45), channel_id=1, source_target_pairs={{0,1},{1,0},{2,3},{3,2},{4,5},{5,4},{6,7},{7,6},{8,9},{9,8},{10,11... | collective-permute-start | bytes 786440 | tf_op jit(solution)/shard_map/ppermute | solution.py:479
  80.5 22.9 %all-to-all-done.1 = bf16[32,16,1024]{2,1,0:T(8,128)(2,1)S(1)} async-done(((bf16[32,16,1024]{2,1,0:T(8,128)(2,1)}), bf16[32,16,1024]{2,1,0:T(8,128)(2,1)S(1)}, u32[]{:S(2)}, u32[]{:S(2)}) %all-to-all-start.1) | async-done | bytes 1048608 | tf_op jit(solution)/shard_map/all_to_all | solution.py:462
  103.4 1.9 %shard_map.210 = bf16[8,128,128]{2,1,0:T(8,128)(2,1)} custom-call(bf16[512,1024]{1,0:T(8,128)(2,1)S(1)} %bitcast.28, bf16[512,128]{1,0:T(8,128)(2,1)} %get-tuple-element.38.weighing), custom_call_target="tpu_custom_call" | custom-call | tf_op jit(solution)/shard_map/pallas_call | solution.py:319
  105.3 7.1 %all-to-all-start.2 = ((bf16[8,128,128]{2,1,0:T(8,128)(2,1)}), bf16[8,128,128]{2,1,0:T(8,128)(2,1)S(1)}, u32[]{:S(2)}, u32[]{:S(2)}) async-start(bf16[8,128,128]{2,1,0:T(8,128)(2,1)} %shard_map.210), calls=%async_computation.2 | async-start | bytes 524288 | tf_op jit(solution)/shard_map/all_to_all | solution.py:500
  112.5 3.9 %collective-permute-start.6 = (bf16[4,8,2048]{2,1,0:T(8,128)(2,1)S(1)}, bf16[4,8,2048]{2,1,0:T(8,128)(2,1)S(1)}, u32[]{:S(2)}, u32[]{:S(2)}) collective-permute-start(bf16[4,8,2048]{2,1,0:T(8,128)(2,1)S(1)} %get-tuple-element.47), channel_id=1, source_target_pairs={{0,2},{1,3},{2,0},{3,1},{4,6},{5,7},{6,4},{7,5},{8,10},{9,11},{10,... | collective-permute-start | bytes 393224 | tf_op jit(solution)/shard_map/ppermute | solution.py:490
  116.5 4.5 %collective-permute-done.6.landed = bf16[4,8,2048]{2,1,0:T(8,128)(2,1)S(1)} collective-permute-done((bf16[4,8,2048]{2,1,0:T(8,128)(2,1)S(1)}, bf16[4,8,2048]{2,1,0:T(8,128)(2,1)S(1)}, u32[]{:S(2)}, u32[]{:S(2)}) %collective-permute-start.6) | collective-permute-done | bytes 131104 | tf_op jit(solution)/shard_map/ppermute | solution.py:490
  121.0 5.2 %collective-permute-start.7 = (bf16[2,8,2048]{2,1,0:T(8,128)(2,1)S(1)}, bf16[2,8,2048]{2,1,0:T(8,128)(2,1)S(1)}, u32[]{:S(2)}, u32[]{:S(2)}) collective-permute-start(bf16[2,8,2048]{2,1,0:T(8,128)(2,1)S(1)} %get-tuple-element.49), channel_id=1, source_target_pairs={{0,4},{1,5},{2,6},{3,7},{4,0},{5,1},{6,2},{7,3},{8,12},{9,13},{10,... | collective-permute-start | bytes 196616 | tf_op jit(solution)/shard_map/ppermute | solution.py:490
  126.2 2.9 %collective-permute-done.7.landed = bf16[2,8,2048]{2,1,0:T(8,128)(2,1)S(1)} collective-permute-done((bf16[2,8,2048]{2,1,0:T(8,128)(2,1)S(1)}, bf16[2,8,2048]{2,1,0:T(8,128)(2,1)S(1)}, u32[]{:S(2)}, u32[]{:S(2)}) %collective-permute-start.7) | collective-permute-done | bytes 65568 | tf_op jit(solution)/shard_map/ppermute | solution.py:490
  129.1 6.0 %collective-permute-start.8 = (bf16[1,8,2048]{2,1,0:T(8,128)(2,1)S(1)}, bf16[1,8,2048]{2,1,0:T(8,128)(2,1)S(1)}, u32[]{:S(2)}, u32[]{:S(2)}) collective-permute-start(bf16[1,8,2048]{2,1,0:T(8,128)(2,1)S(1)} %get-tuple-element.51), channel_id=1, source_target_pairs={{0,8},{1,9},{2,10},{3,11},{4,12},{5,13},{6,14},{7,15},{8,0},{9,1},... | collective-permute-start | bytes 98312 | tf_op jit(solution)/shard_map/ppermute | solution.py:490
  135.2 3.8 %collective-permute-done.8.landed = bf16[1,8,2048]{2,1,0:T(8,128)(2,1)S(1)} collective-permute-done((bf16[1,8,2048]{2,1,0:T(8,128)(2,1)S(1)}, bf16[1,8,2048]{2,1,0:T(8,128)(2,1)S(1)}, u32[]{:S(2)}, u32[]{:S(2)}) %collective-permute-start.8) | collective-permute-done | bytes 32800 | tf_op jit(solution)/shard_map/ppermute | solution.py:490
  139.0 0.7 shard_map.215
  (11 shorter events, 0.2 us)
Async XLA Ops:
  3.4 42.6 %all-to-all-start = ((bf16[32,16,1024]{2,1,0:T(8,128)(2,1)}), bf16[32,16,1024]{2,1,0:T(8,128)(2,1)S(1)}, u32[]{:S(2)}, u32[]{:S(2)}) async-start(bf16[32,16,1024]{2,1,0:T(8,128)(2,1)} %bitcast.4), calls=%async_computation | async-start | bytes 2097152 | tf_op jit(solution)/shard_map/all_to_all | solution.py:377
  19.6 31.0 %copy-start = (bf16[1,2048,256]{2,1,0:T(8,128)(2,1)S(1)}, bf16[1,2048,256]{2,1,0:T(8,128)(2,1)}, u32[]{:S(2)}) copy-start(bf16[1,2048,256]{2,1,0:T(8,128)(2,1)} %param.38) | copy-start | bytes 3145732
  19.6 26.4 %collective-permute-start.2 = (bf16[256,1024]{1,0:T(8,128)(2,1)}, bf16[256,1024]{1,0:T(8,128)(2,1)}, u32[]{:S(2)}, u32[]{:S(2)}) collective-permute-start(bf16[256,1024]{1,0:T(8,128)(2,1)} %get-tuple-element.33), channel_id=1, source_target_pairs={{0,1},{1,0},{2,3},{3,2},{4,5},{5,4},{6,7},{7,6},{8,9},{9,8},{10,11... | collective-permute-start | bytes 1572872 | tf_op jit(solution)/shard_map/ppermute | solution.py:428
  30.1 6.2 %collective-permute-start = (bf16[128,128]{1,0:T(8,128)(2,1)S(1)}, bf16[128,128]{1,0:T(8,128)(2,1)S(1)}, u32[]{:S(2)}, u32[]{:S(2)}) collective-permute-start(bf16[128,128]{1,0:T(8,128)(2,1)S(1)} %get-tuple-element.28.mine), channel_id=1, source_target_pairs={{0,16},{16,0},{32,48},{48,32},{64,80},{80,64},{96,112},{112,96},{1... | collective-permute-start | bytes 98312 | tf_op jit(solution)/shard_map/ppermute | solution.py:357
  37.1 7.3 %collective-permute-start.1 = (bf16[128,128]{1,0:T(8,128)(2,1)S(1)}, bf16[128,128]{1,0:T(8,128)(2,1)S(1)}, u32[]{:S(2)}, u32[]{:S(2)}) collective-permute-start(bf16[128,128]{1,0:T(8,128)(2,1)S(1)} %get-tuple-element.29.mine), channel_id=1, source_target_pairs={{0,32},{16,48},{32,0},{48,16},{64,96},{80,112},{96,64},{112,80},{1... | collective-permute-start | bytes 98312 | tf_op jit(solution)/shard_map/ppermute | solution.py:357
  46.0 4.6 %collective-permute-start.3 = (bf16[512,1024]{1,0:T(8,128)(2,1)S(1)}, bf16[512,1024]{1,0:T(8,128)(2,1)S(1)}, u32[]{:S(2)}, u32[]{:S(2)}) collective-permute-start(bf16[512,1024]{1,0:T(8,128)(2,1)S(1)} %bitcast.26), channel_id=1, source_target_pairs={{0,1},{1,0},{2,3},{3,2},{4,5},{5,4},{6,7},{7,6},{8,9},{9,8},{10,11... | collective-permute-start | bytes 3145736 | tf_op jit(solution)/shard_map/ppermute | solution.py:441
  51.9 9.5 %collective-permute-start.4 = (bf16[512,256]{1,0:T(8,128)(2,1)S(1)}, bf16[512,256]{1,0:T(8,128)(2,1)S(1)}, u32[]{:S(2)}, u32[]{:S(2)}) collective-permute-start(bf16[512,256]{1,0:T(8,128)(2,1)S(1)} %shard_map.208.hidden), channel_id=1, source_target_pairs={{0,1},{1,0},{2,3},{3,2},{4,5},{5,4},{6,7},{7,6},{8,9},{9,8},{10,11... | collective-permute-start | bytes 786440 | tf_op jit(solution)/shard_map/ppermute | solution.py:451
  53.9 17.1 %all-to-all-start.3 = ((bf16[8,64,128]{2,1,0:T(8,128)(2,1)}), bf16[8,64,128]{2,1,0:T(8,128)(2,1)S(1)}, u32[]{:S(2)}, u32[]{:S(2)}) async-start(bf16[8,64,128]{2,1,0:T(8,128)(2,1)} %get-tuple-element.39), calls=%async_computation.3 | async-start | bytes 262144 | tf_op jit(solution)/shard_map/all_to_all | solution.py:432
  61.4 1.0 copy-start.1
  71.0 32.4 %all-to-all-start.1 = ((bf16[32,16,1024]{2,1,0:T(8,128)(2,1)}), bf16[32,16,1024]{2,1,0:T(8,128)(2,1)S(1)}, u32[]{:S(2)}, u32[]{:S(2)}) async-start(bf16[32,16,1024]{2,1,0:T(8,128)(2,1)} %bitcast.20), calls=%async_computation.1 | async-start | bytes 2097152 | tf_op jit(solution)/shard_map/all_to_all | solution.py:462
  78.5 33.9 %collective-permute-start.5 = (bf16[8,8,2048]{2,1,0:T(8,128)(2,1)S(1)}, bf16[8,8,2048]{2,1,0:T(8,128)(2,1)S(1)}, u32[]{:S(2)}, u32[]{:S(2)}) collective-permute-start(bf16[8,8,2048]{2,1,0:T(8,128)(2,1)S(1)} %get-tuple-element.45), channel_id=1, source_target_pairs={{0,1},{1,0},{2,3},{3,2},{4,5},{5,4},{6,7},{7,6},{8,9},{9,8},{10,11... | collective-permute-start | bytes 786440 | tf_op jit(solution)/shard_map/ppermute | solution.py:479
  105.3 33.6 %all-to-all-start.2 = ((bf16[8,128,128]{2,1,0:T(8,128)(2,1)}), bf16[8,128,128]{2,1,0:T(8,128)(2,1)S(1)}, u32[]{:S(2)}, u32[]{:S(2)}) async-start(bf16[8,128,128]{2,1,0:T(8,128)(2,1)} %shard_map.210), calls=%async_computation.2 | async-start | bytes 524288 | tf_op jit(solution)/shard_map/all_to_all | solution.py:500
  112.5 8.4 %collective-permute-start.6 = (bf16[4,8,2048]{2,1,0:T(8,128)(2,1)S(1)}, bf16[4,8,2048]{2,1,0:T(8,128)(2,1)S(1)}, u32[]{:S(2)}, u32[]{:S(2)}) collective-permute-start(bf16[4,8,2048]{2,1,0:T(8,128)(2,1)S(1)} %get-tuple-element.47), channel_id=1, source_target_pairs={{0,2},{1,3},{2,0},{3,1},{4,6},{5,7},{6,4},{7,5},{8,10},{9,11},{10,... | collective-permute-start | bytes 393224 | tf_op jit(solution)/shard_map/ppermute | solution.py:490
  121.0 8.1 %collective-permute-start.7 = (bf16[2,8,2048]{2,1,0:T(8,128)(2,1)S(1)}, bf16[2,8,2048]{2,1,0:T(8,128)(2,1)S(1)}, u32[]{:S(2)}, u32[]{:S(2)}) collective-permute-start(bf16[2,8,2048]{2,1,0:T(8,128)(2,1)S(1)} %get-tuple-element.49), channel_id=1, source_target_pairs={{0,4},{1,5},{2,6},{3,7},{4,0},{5,1},{6,2},{7,3},{8,12},{9,13},{10,... | collective-permute-start | bytes 196616 | tf_op jit(solution)/shard_map/ppermute | solution.py:490
  129.1 9.8 %collective-permute-start.8 = (bf16[1,8,2048]{2,1,0:T(8,128)(2,1)S(1)}, bf16[1,8,2048]{2,1,0:T(8,128)(2,1)S(1)}, u32[]{:S(2)}, u32[]{:S(2)}) collective-permute-start(bf16[1,8,2048]{2,1,0:T(8,128)(2,1)S(1)} %get-tuple-element.51), channel_id=1, source_target_pairs={{0,8},{1,9},{2,10},{3,11},{4,12},{5,13},{6,14},{7,15},{8,0},{9,1},... | collective-permute-start | bytes 98312 | tf_op jit(solution)/shard_map/ppermute | solution.py:490

commit v5 on v4

--- a/solution.py
+++ b/solution.py
@@ -367,7 +367,7 @@
 
     buffer, weighing = call(
         functools.partial(dispatch_kernel, experts, slots),
-        (shape((experts * slots, half), BF16), far(shape((experts * slots, tokens), BF16))),
+        (shape((experts * slots, half), BF16), near(shape((experts * slots, tokens), BF16))),
         (scalar(core),),
         far(moe_rows),
         far(moe_gain.reshape(1, -1)),
@@ -474,7 +474,7 @@
         far(reads_f),
         far(reads_b),
         far(out_gain.reshape(1, -1)),
-        far(w_output),
+        near(w_output),
     )
     keep, landed = (own_rows, lax.ppermute(away_rows, "tp", swap))
     bit = 1
@@ -495,7 +495,7 @@
         near(shape((chips, tokens, piece), BF16)),
         (),
         near(returned),
-        far(weighing),
+        near(weighing),
     )
     parts = lax.all_to_all(
         parts,

time: 141 us -> 140 us (level)
  no operation moved by 1% of the time
where the time goes in v5:
time: 140 us; the launch traced here: 139 us
  starting transfers between devices  62.2 us (44%)
  waiting for transfers between devices  49.8 us (36%)
  Pallas kernels  25 us (18%)
    pallas_call x13, Pallas kernels, call(): pl.pallas_call(kernel, out_shape=outs, in_specs=[smem] * len(scalars) + [...  25 us
    all_to_all x1, waiting for transfers between devices, shards(): lax.all_to_all(paired.reshape(experts, slots, half), 'ep', split_axis=0,...  23.1 us
    ppermute x3, starting transfers between devices, shards(): landed = lax.ppermute(send, 'tp', [(k, k ^ 2 * bit) for k in range(tp)])  15.2 us
    all_to_all x1, starting transfers between devices, shards(): lax.all_to_all(buffer.reshape(experts, slots, half), 'ep', split_axis=0,...  13.4 us
    ppermute x3, waiting for transfers between devices, shards(): landed = lax.ppermute(send, 'tp', [(k, k ^ 2 * bit) for k in range(tp)])  11.2 us
    all_to_all x1, starting transfers between devices, shards(): lax.all_to_all(sent, 'ep', split_axis=0, concat_axis=0, tiled=True, axis_...  7.49 us
    ppermute x2, waiting for transfers between devices, shards(): lax.ppermute(value, 'ep', [(k, k ^ bit) for k in range(experts)])  7.13 us
    all_to_all x1, starting transfers between devices, shards(): lax.all_to_all(parts, 'tp', split_axis=0, concat_axis=0, tiled=True, axis...  7.11 us
  transfers between devices with their start and end apart: 13, of which 8 were waited for; matrix products, arithmetic and copies ran while one was open for 0% of the time, Pallas kernels for 15%

profile of v5, /device:TPU:6, one launch (start us, length us, event | category | flops | bytes accessed | tf_op | source)
XLA Modules:
  0.0 138.9 jit_solution(14441337489616223532)
XLA Ops:
  0.6 2.7 %shard_map.203 = (bf16[512,1024]{1,0:T(8,128)(2,1)}, bf16[512,128]{1,0:T(8,128)(2,1)S(1)}) custom-call(s32[1]{0:T(128)} %bitcast.core, bf16[128,2048]{1,0:T(8,128)(2,1)} %rows.1, f32[1,2048]{1,0:T(1,128)} %bitcast.36, s32[2,128]{1,0:T(2,128)} %bitcast.38, f32[2,128]{1,0:T(2,128)} %bitcast.39), custom_call_target="tpu_custom_call" | custom-call | tf_op jit(solution)/shard_map/pallas_call | solution.py:319
  3.4 13.4 %all-to-all-start = ((bf16[32,16,1024]{2,1,0:T(8,128)(2,1)}), bf16[32,16,1024]{2,1,0:T(8,128)(2,1)S(1)}, u32[]{:S(2)}, u32[]{:S(2)}) async-start(bf16[32,16,1024]{2,1,0:T(8,128)(2,1)} %bitcast.4), calls=%async_computation | async-start | bytes 2097152 | tf_op jit(solution)/shard_map/all_to_all | solution.py:377
  16.8 2.8 %shard_map.207 = (bf16[2048,256]{1,0:T(8,128)(2,1)S(1)}, bf16[256,1024]{1,0:T(8,128)(2,1)}, bf16[256,1024]{1,0:T(8,128)(2,1)}) custom-call(s32[1]{0:T(128)} %bitcast.core, bf16[2048,256]{1,0:T(8,128)(2,1)} %bitcast.30, bf16[256,2048]{1,0:T(8,128)(2,1)} %bitcast.31), custom_call_target="tpu_custom_call" | custom-call | tf_op jit(solution)/shard_map/pallas_call | solution.py:319
  19.5 2.0 %collective-permute-start.2 = (bf16[256,1024]{1,0:T(8,128)(2,1)}, bf16[256,1024]{1,0:T(8,128)(2,1)}, u32[]{:S(2)}, u32[]{:S(2)}) collective-permute-start(bf16[256,1024]{1,0:T(8,128)(2,1)} %get-tuple-element.33), channel_id=1, source_target_pairs={{0,1},{1,0},{2,3},{3,2},{4,5},{5,4},{6,7},{7,6},{8,9},{9,8},{10,11... | collective-permute-start | bytes 1572872 | tf_op jit(solution)/shard_map/ppermute | solution.py:428
  21.6 8.5 %shard_map.204 = (f32[128,128]{1,0:T(8,128)}, f32[128,128]{1,0:T(8,128)}, bf16[128,128]{1,0:T(8,128)(2,1)S(1)}) custom-call(bf16[128,2048]{1,0:T(8,128)(2,1)} %refs_0_.1, f32[1,2048]{1,0:T(1,128)} %bitcast.37, bf16[64,2048]{1,0:T(8,128)(2,1)} %bitcast.32, bf16[64,2048]{1,0:T(8,128)(2,1)} %bitcast.33, bf16[64,2048]{1,0:T(8,128)(2,1)} %bitcast.34, ...), custom_call_target="tpu_custom_call" | custom-call | tf_op jit(solution)/shard_map/pallas_call | solution.py:319
  30.1 2.8 %collective-permute-start = (bf16[128,128]{1,0:T(8,128)(2,1)S(1)}, bf16[128,128]{1,0:T(8,128)(2,1)S(1)}, u32[]{:S(2)}, u32[]{:S(2)}) collective-permute-start(bf16[128,128]{1,0:T(8,128)(2,1)S(1)} %get-tuple-element.28.mine), channel_id=1, source_target_pairs={{0,16},{16,0},{32,48},{48,32},{64,80},{80,64},{96,112},{112,96},{1... | collective-permute-start | bytes 98312 | tf_op jit(solution)/shard_map/ppermute | solution.py:357
  32.9 3.4 %collective-permute-done.theirs = bf16[128,128]{1,0:T(8,128)(2,1)S(1)} collective-permute-done((bf16[128,128]{1,0:T(8,128)(2,1)S(1)}, bf16[128,128]{1,0:T(8,128)(2,1)S(1)}, u32[]{:S(2)}, u32[]{:S(2)}) %collective-permute-start) | collective-permute-done | bytes 32800 | tf_op jit(solution)/shard_map/ppermute | solution.py:357
  36.3 0.8 shard_map.205
  37.1 3.6 %collective-permute-start.1 = (bf16[128,128]{1,0:T(8,128)(2,1)S(1)}, bf16[128,128]{1,0:T(8,128)(2,1)S(1)}, u32[]{:S(2)}, u32[]{:S(2)}) collective-permute-start(bf16[128,128]{1,0:T(8,128)(2,1)S(1)} %get-tuple-element.29.mine), channel_id=1, source_target_pairs={{0,32},{16,48},{32,0},{48,16},{64,96},{80,112},{96,64},{112,80},{1... | collective-permute-start | bytes 98312 | tf_op jit(solution)/shard_map/ppermute | solution.py:357
  40.7 3.7 %collective-permute-done.1.theirs = bf16[128,128]{1,0:T(8,128)(2,1)S(1)} collective-permute-done((bf16[128,128]{1,0:T(8,128)(2,1)S(1)}, bf16[128,128]{1,0:T(8,128)(2,1)S(1)}, u32[]{:S(2)}, u32[]{:S(2)}) %collective-permute-start.1) | collective-permute-done | bytes 32800 | tf_op jit(solution)/shard_map/ppermute | solution.py:357
  44.4 1.6 %shard_map.206 = (bf16[8,64,128]{2,1,0:T(8,128)(2,1)}, f32[64,128]{1,0:T(8,128)}, f32[64,128]{1,0:T(8,128)}) custom-call(s32[1]{0:T(128)} %bitcast.6.high, s32[1]{0:T(128)} %bitcast.7.run, bf16[128,128]{1,0:T(8,128)(2,1)S(1)} %get-tuple-element.29.mine, bf16[128,128]{1,0:T(8,128)(2,1)S(1)} %collective-permute-done.1.theirs, ...), custom_call_target="tpu_custom_call" | custom-call | tf_op jit(solution)/shard_map/pallas_call | solution.py:319
  46.0 1.9 %collective-permute-start.3 = (bf16[512,1024]{1,0:T(8,128)(2,1)S(1)}, bf16[512,1024]{1,0:T(8,128)(2,1)S(1)}, u32[]{:S(2)}, u32[]{:S(2)}) collective-permute-start(bf16[512,1024]{1,0:T(8,128)(2,1)S(1)} %bitcast.26), channel_id=1, source_target_pairs={{0,1},{1,0},{2,3},{3,2},{4,5},{5,4},{6,7},{7,6},{8,9},{9,8},{10,11... | collective-permute-start | bytes 3145736 | tf_op jit(solution)/shard_map/ppermute | solution.py:441
  48.0 2.6 %collective-permute-done.3.swapped = bf16[512,1024]{1,0:T(8,128)(2,1)S(1)} collective-permute-done((bf16[512,1024]{1,0:T(8,128)(2,1)S(1)}, bf16[512,1024]{1,0:T(8,128)(2,1)S(1)}, u32[]{:S(2)}, u32[]{:S(2)}) %collective-permute-start.3) | collective-permute-done | bytes 1048608 | tf_op jit(solution)/shard_map/ppermute | solution.py:441
  50.6 1.3 shard_map.208.hidden
  51.9 2.0 %collective-permute-start.4 = (bf16[512,256]{1,0:T(8,128)(2,1)S(1)}, bf16[512,256]{1,0:T(8,128)(2,1)S(1)}, u32[]{:S(2)}, u32[]{:S(2)}) collective-permute-start(bf16[512,256]{1,0:T(8,128)(2,1)S(1)} %shard_map.208.hidden), channel_id=1, source_target_pairs={{0,1},{1,0},{2,3},{3,2},{4,5},{5,4},{6,7},{7,6},{8,9},{9,8},{10,11... | collective-permute-start | bytes 786440 | tf_op jit(solution)/shard_map/ppermute | solution.py:451
  53.9 7.5 %all-to-all-start.3 = ((bf16[8,64,128]{2,1,0:T(8,128)(2,1)}), bf16[8,64,128]{2,1,0:T(8,128)(2,1)S(1)}, u32[]{:S(2)}, u32[]{:S(2)}) async-start(bf16[8,64,128]{2,1,0:T(8,128)(2,1)} %get-tuple-element.39), calls=%async_computation.3 | async-start | bytes 262144 | tf_op jit(solution)/shard_map/all_to_all | solution.py:432
  61.4 1.0 copy-done.1
  62.5 2.8 %shard_map.209 = bf16[512,1024]{1,0:T(8,128)(2,1)} custom-call(bf16[512,256]{1,0:T(8,128)(2,1)S(1)} %shard_map.208.hidden, bf16[512,256]{1,0:T(8,128)(2,1)S(1)} %collective-permute-done.4.landed, bf16[256,1024]{1,0:T(8,128)(2,1)S(1)} %copy-done.1, bf16[256,1024]{1,0:T(8,128)(2,1)} %collective-permute-done.2.other), custom_call_target="tpu_custom_call" | custom-call | tf_op jit(solution)/shard_map/pallas_call | solution.py:319
  65.2 5.8 %all-to-all-done.3.arrived = bf16[8,64,128]{2,1,0:T(8,128)(2,1)S(1)} async-done(((bf16[8,64,128]{2,1,0:T(8,128)(2,1)}), bf16[8,64,128]{2,1,0:T(8,128)(2,1)S(1)}, u32[]{:S(2)}, u32[]{:S(2)}) %all-to-all-start.3) | async-done | bytes 131104 | tf_op jit(solution)/shard_map/all_to_all | solution.py:432
  71.0 4.8 %all-to-all-start.1 = ((bf16[32,16,1024]{2,1,0:T(8,128)(2,1)}), bf16[32,16,1024]{2,1,0:T(8,128)(2,1)S(1)}, u32[]{:S(2)}, u32[]{:S(2)}) async-start(bf16[32,16,1024]{2,1,0:T(8,128)(2,1)} %bitcast.20), calls=%async_computation.1 | async-start | bytes 2097152 | tf_op jit(solution)/shard_map/all_to_all | solution.py:462
  75.9 2.7 %shard_map.211 = (bf16[8,8,2048]{2,1,0:T(8,128)(2,1)S(1)}, bf16[8,8,2048]{2,1,0:T(8,128)(2,1)S(1)}) custom-call(s32[1]{0:T(128)} %bitcast.7.run, s32[1]{0:T(128)} %bitcast.core, bf16[8,64,128]{2,1,0:T(8,128)(2,1)S(1)} %all-to-all-done.3.arrived, f32[64,128]{1,0:T(8,128)} %get-tuple-element.40.before, f32[64,128]{1,0:T(8,128)} %get-tuple-element.41.after, ...), custom_call_target="tpu_custom_call" | custom-call | tf_op jit(solution)/shard_map/pallas_call | solution.py:319
  78.6 1.9 %collective-permute-start.5 = (bf16[8,8,2048]{2,1,0:T(8,128)(2,1)S(1)}, bf16[8,8,2048]{2,1,0:T(8,128)(2,1)S(1)}, u32[]{:S(2)}, u32[]{:S(2)}) collective-permute-start(bf16[8,8,2048]{2,1,0:T(8,128)(2,1)S(1)} %get-tuple-element.45), channel_id=1, source_target_pairs={{0,1},{1,0},{2,3},{3,2},{4,5},{5,4},{6,7},{7,6},{8,9},{9,8},{10,11... | collective-permute-start | bytes 786440 | tf_op jit(solution)/shard_map/ppermute | solution.py:479
  80.5 23.1 %all-to-all-done.1 = bf16[32,16,1024]{2,1,0:T(8,128)(2,1)S(1)} async-done(((bf16[32,16,1024]{2,1,0:T(8,128)(2,1)}), bf16[32,16,1024]{2,1,0:T(8,128)(2,1)S(1)}, u32[]{:S(2)}, u32[]{:S(2)}) %all-to-all-start.1) | async-done | bytes 1048608 | tf_op jit(solution)/shard_map/all_to_all | solution.py:462
  103.6 1.0 shard_map.210
  104.6 7.1 %all-to-all-start.2 = ((bf16[8,128,128]{2,1,0:T(8,128)(2,1)}), bf16[8,128,128]{2,1,0:T(8,128)(2,1)S(1)}, u32[]{:S(2)}, u32[]{:S(2)}) async-start(bf16[8,128,128]{2,1,0:T(8,128)(2,1)} %shard_map.210), calls=%async_computation.2 | async-start | bytes 524288 | tf_op jit(solution)/shard_map/all_to_all | solution.py:500
  111.8 3.9 %collective-permute-start.6 = (bf16[4,8,2048]{2,1,0:T(8,128)(2,1)S(1)}, bf16[4,8,2048]{2,1,0:T(8,128)(2,1)S(1)}, u32[]{:S(2)}, u32[]{:S(2)}) collective-permute-start(bf16[4,8,2048]{2,1,0:T(8,128)(2,1)S(1)} %get-tuple-element.47), channel_id=1, source_target_pairs={{0,2},{1,3},{2,0},{3,1},{4,6},{5,7},{6,4},{7,5},{8,10},{9,11},{10,... | collective-permute-start | bytes 393224 | tf_op jit(solution)/shard_map/ppermute | solution.py:490
  115.7 4.5 %collective-permute-done.6.landed = bf16[4,8,2048]{2,1,0:T(8,128)(2,1)S(1)} collective-permute-done((bf16[4,8,2048]{2,1,0:T(8,128)(2,1)S(1)}, bf16[4,8,2048]{2,1,0:T(8,128)(2,1)S(1)}, u32[]{:S(2)}, u32[]{:S(2)}) %collective-permute-start.6) | collective-permute-done | bytes 131104 | tf_op jit(solution)/shard_map/ppermute | solution.py:490
  120.3 5.2 %collective-permute-start.7 = (bf16[2,8,2048]{2,1,0:T(8,128)(2,1)S(1)}, bf16[2,8,2048]{2,1,0:T(8,128)(2,1)S(1)}, u32[]{:S(2)}, u32[]{:S(2)}) collective-permute-start(bf16[2,8,2048]{2,1,0:T(8,128)(2,1)S(1)} %get-tuple-element.49), channel_id=1, source_target_pairs={{0,4},{1,5},{2,6},{3,7},{4,0},{5,1},{6,2},{7,3},{8,12},{9,13},{10,... | collective-permute-start | bytes 196616 | tf_op jit(solution)/shard_map/ppermute | solution.py:490
  125.5 2.9 %collective-permute-done.7.landed = bf16[2,8,2048]{2,1,0:T(8,128)(2,1)S(1)} collective-permute-done((bf16[2,8,2048]{2,1,0:T(8,128)(2,1)S(1)}, bf16[2,8,2048]{2,1,0:T(8,128)(2,1)S(1)}, u32[]{:S(2)}, u32[]{:S(2)}) %collective-permute-start.7) | collective-permute-done | bytes 65568 | tf_op jit(solution)/shard_map/ppermute | solution.py:490
  128.4 6.0 %collective-permute-start.8 = (bf16[1,8,2048]{2,1,0:T(8,128)(2,1)S(1)}, bf16[1,8,2048]{2,1,0:T(8,128)(2,1)S(1)}, u32[]{:S(2)}, u32[]{:S(2)}) collective-permute-start(bf16[1,8,2048]{2,1,0:T(8,128)(2,1)S(1)} %get-tuple-element.51), channel_id=1, source_target_pairs={{0,8},{1,9},{2,10},{3,11},{4,12},{5,13},{6,14},{7,15},{8,0},{9,1},... | collective-permute-start | bytes 98312 | tf_op jit(solution)/shard_map/ppermute | solution.py:490
  134.5 3.8 %collective-permute-done.8.landed = bf16[1,8,2048]{2,1,0:T(8,128)(2,1)S(1)} collective-permute-done((bf16[1,8,2048]{2,1,0:T(8,128)(2,1)S(1)}, bf16[1,8,2048]{2,1,0:T(8,128)(2,1)S(1)}, u32[]{:S(2)}, u32[]{:S(2)}) %collective-permute-start.8) | collective-permute-done | bytes 32800 | tf_op jit(solution)/shard_map/ppermute | solution.py:490
  138.2 0.7 shard_map.215
  (13 shorter events, 0.2 us)
Async XLA Ops:
  3.4 42.7 %all-to-all-start = ((bf16[32,16,1024]{2,1,0:T(8,128)(2,1)}), bf16[32,16,1024]{2,1,0:T(8,128)(2,1)S(1)}, u32[]{:S(2)}, u32[]{:S(2)}) async-start(bf16[32,16,1024]{2,1,0:T(8,128)(2,1)} %bitcast.4), calls=%async_computation | async-start | bytes 2097152 | tf_op jit(solution)/shard_map/all_to_all | solution.py:377
  19.5 31.1 %copy-start = (bf16[1,2048,256]{2,1,0:T(8,128)(2,1)S(1)}, bf16[1,2048,256]{2,1,0:T(8,128)(2,1)}, u32[]{:S(2)}) copy-start(bf16[1,2048,256]{2,1,0:T(8,128)(2,1)} %param.38) | copy-start | bytes 3145732
  19.5 26.5 %collective-permute-start.2 = (bf16[256,1024]{1,0:T(8,128)(2,1)}, bf16[256,1024]{1,0:T(8,128)(2,1)}, u32[]{:S(2)}, u32[]{:S(2)}) collective-permute-start(bf16[256,1024]{1,0:T(8,128)(2,1)} %get-tuple-element.33), channel_id=1, source_target_pairs={{0,1},{1,0},{2,3},{3,2},{4,5},{5,4},{6,7},{7,6},{8,9},{9,8},{10,11... | collective-permute-start | bytes 1572872 | tf_op jit(solution)/shard_map/ppermute | solution.py:428
  30.1 6.2 %collective-permute-start = (bf16[128,128]{1,0:T(8,128)(2,1)S(1)}, bf16[128,128]{1,0:T(8,128)(2,1)S(1)}, u32[]{:S(2)}, u32[]{:S(2)}) collective-permute-start(bf16[128,128]{1,0:T(8,128)(2,1)S(1)} %get-tuple-element.28.mine), channel_id=1, source_target_pairs={{0,16},{16,0},{32,48},{48,32},{64,80},{80,64},{96,112},{112,96},{1... | collective-permute-start | bytes 98312 | tf_op jit(solution)/shard_map/ppermute | solution.py:357
  37.1 7.3 %collective-permute-start.1 = (bf16[128,128]{1,0:T(8,128)(2,1)S(1)}, bf16[128,128]{1,0:T(8,128)(2,1)S(1)}, u32[]{:S(2)}, u32[]{:S(2)}) collective-permute-start(bf16[128,128]{1,0:T(8,128)(2,1)S(1)} %get-tuple-element.29.mine), channel_id=1, source_target_pairs={{0,32},{16,48},{32,0},{48,16},{64,96},{80,112},{96,64},{112,80},{1... | collective-permute-start | bytes 98312 | tf_op jit(solution)/shard_map/ppermute | solution.py:357
  46.0 4.6 %collective-permute-start.3 = (bf16[512,1024]{1,0:T(8,128)(2,1)S(1)}, bf16[512,1024]{1,0:T(8,128)(2,1)S(1)}, u32[]{:S(2)}, u32[]{:S(2)}) collective-permute-start(bf16[512,1024]{1,0:T(8,128)(2,1)S(1)} %bitcast.26), channel_id=1, source_target_pairs={{0,1},{1,0},{2,3},{3,2},{4,5},{5,4},{6,7},{7,6},{8,9},{9,8},{10,11... | collective-permute-start | bytes 3145736 | tf_op jit(solution)/shard_map/ppermute | solution.py:441
  51.9 9.5 %collective-permute-start.4 = (bf16[512,256]{1,0:T(8,128)(2,1)S(1)}, bf16[512,256]{1,0:T(8,128)(2,1)S(1)}, u32[]{:S(2)}, u32[]{:S(2)}) collective-permute-start(bf16[512,256]{1,0:T(8,128)(2,1)S(1)} %shard_map.208.hidden), channel_id=1, source_target_pairs={{0,1},{1,0},{2,3},{3,2},{4,5},{5,4},{6,7},{7,6},{8,9},{9,8},{10,11... | collective-permute-start | bytes 786440 | tf_op jit(solution)/shard_map/ppermute | solution.py:451
  53.9 17.1 %all-to-all-start.3 = ((bf16[8,64,128]{2,1,0:T(8,128)(2,1)}), bf16[8,64,128]{2,1,0:T(8,128)(2,1)S(1)}, u32[]{:S(2)}, u32[]{:S(2)}) async-start(bf16[8,64,128]{2,1,0:T(8,128)(2,1)} %get-tuple-element.39), calls=%async_computation.3 | async-start | bytes 262144 | tf_op jit(solution)/shard_map/all_to_all | solution.py:432
  61.4 1.0 copy-start.1
  71.0 4.8 %copy-start.2 = (bf16[64,2048]{1,0:T(8,128)(2,1)S(1)}, bf16[64,2048]{1,0:T(8,128)(2,1)}, u32[]{:S(2)}) copy-start(bf16[64,2048]{1,0:T(8,128)(2,1)} %w_output.1) | copy-start | bytes 786436
  71.0 32.5 %all-to-all-start.1 = ((bf16[32,16,1024]{2,1,0:T(8,128)(2,1)}), bf16[32,16,1024]{2,1,0:T(8,128)(2,1)S(1)}, u32[]{:S(2)}, u32[]{:S(2)}) async-start(bf16[32,16,1024]{2,1,0:T(8,128)(2,1)} %bitcast.20), calls=%async_computation.1 | async-start | bytes 2097152 | tf_op jit(solution)/shard_map/all_to_all | solution.py:462
  78.6 33.2 %collective-permute-start.5 = (bf16[8,8,2048]{2,1,0:T(8,128)(2,1)S(1)}, bf16[8,8,2048]{2,1,0:T(8,128)(2,1)S(1)}, u32[]{:S(2)}, u32[]{:S(2)}) collective-permute-start(bf16[8,8,2048]{2,1,0:T(8,128)(2,1)S(1)} %get-tuple-element.45), channel_id=1, source_target_pairs={{0,1},{1,0},{2,3},{3,2},{4,5},{5,4},{6,7},{7,6},{8,9},{9,8},{10,11... | collective-permute-start | bytes 786440 | tf_op jit(solution)/shard_map/ppermute | solution.py:479
  104.6 33.6 %all-to-all-start.2 = ((bf16[8,128,128]{2,1,0:T(8,128)(2,1)}), bf16[8,128,128]{2,1,0:T(8,128)(2,1)S(1)}, u32[]{:S(2)}, u32[]{:S(2)}) async-start(bf16[8,128,128]{2,1,0:T(8,128)(2,1)} %shard_map.210), calls=%async_computation.2 | async-start | bytes 524288 | tf_op jit(solution)/shard_map/all_to_all | solution.py:500
  111.8 8.4 %collective-permute-start.6 = (bf16[4,8,2048]{2,1,0:T(8,128)(2,1)S(1)}, bf16[4,8,2048]{2,1,0:T(8,128)(2,1)S(1)}, u32[]{:S(2)}, u32[]{:S(2)}) collective-permute-start(bf16[4,8,2048]{2,1,0:T(8,128)(2,1)S(1)} %get-tuple-element.47), channel_id=1, source_target_pairs={{0,2},{1,3},{2,0},{3,1},{4,6},{5,7},{6,4},{7,5},{8,10},{9,11},{10,... | collective-permute-start | bytes 393224 | tf_op jit(solution)/shard_map/ppermute | solution.py:490
  120.3 8.1 %collective-permute-start.7 = (bf16[2,8,2048]{2,1,0:T(8,128)(2,1)S(1)}, bf16[2,8,2048]{2,1,0:T(8,128)(2,1)S(1)}, u32[]{:S(2)}, u32[]{:S(2)}) collective-permute-start(bf16[2,8,2048]{2,1,0:T(8,128)(2,1)S(1)} %get-tuple-element.49), channel_id=1, source_target_pairs={{0,4},{1,5},{2,6},{3,7},{4,0},{5,1},{6,2},{7,3},{8,12},{9,13},{10,... | collective-permute-start | bytes 196616 | tf_op jit(solution)/shard_map/ppermute | solution.py:490
  128.4 9.8 %collective-permute-start.8 = (bf16[1,8,2048]{2,1,0:T(8,128)(2,1)S(1)}, bf16[1,8,2048]{2,1,0:T(8,128)(2,1)S(1)}, u32[]{:S(2)}, u32[]{:S(2)}) collective-permute-start(bf16[1,8,2048]{2,1,0:T(8,128)(2,1)S(1)} %get-tuple-element.51), channel_id=1, source_target_pairs={{0,8},{1,9},{2,10},{3,11},{4,12},{5,13},{6,14},{7,15},{8,0},{9,1},... | collective-permute-start | bytes 98312 | tf_op jit(solution)/shard_map/ppermute | solution.py:490
